TPU v7x, 32 devices: a whole 2x2x4 slice. The times are simulated.
32 devices in a mesh: grp: 2 (over y), sp: 4 (over z), tp: 4 (over x, core).
Axes of the slice: x: 2, y: 2, z: 4, core: 2. Of those that a mesh axis runs over, the one named last changes fastest.
Arguments:
- tokens_in: bfloat16 [2048, 2048], P(('grp', 'sp'), 'tp'), parts along dimension 0, may hold values from -6 to 6
- norm_gain: float32 [3, 2048], replicated, may hold values from 0.1 to 1.9
- w_pool_in: bfloat16 [3, 2048, 1024], P(None, 'sp', 'tp'), may hold values from -0.125 to 0.125
- w_gate: bfloat16 [3, 2048, 2048], P(None, 'sp', 'tp'), may hold values from -0.125 to 0.125
- w_back: bfloat16 [3, 1024, 2048], P(None, 'tp', 'sp'), may hold values from -0.25 to 0.25
Outputs:
- tokens_out: bfloat16 [2048, 2048], P(('grp', 'sp'), 'tp'), parts along dimension 0
There are 2 independent parts, one for each index of `grp`. A program takes and returns all parts, laid end to end along the dimension named above; an argument that names none is the same for every part. Nothing has to cross between parts.
All inputs are finite; a program needn't handle non-finite values.
Results may differ from a plain program's by a relative error of at most 0.017.
Values may be sent and summed in bfloat16 or wider, within the bound.
A program may use at most 64 MiB of HBM per device.

v0:
```python
import jax
import jax.numpy as jnp
from jax import lax
from jax.experimental import pallas as pl
from jax.experimental.pallas import tpu as pltpu
from jax.sharding import PartitionSpec as P
import functools

POOL_WIDTH = 1024
GROUPS = 4
GRID_W = 32
LAYERS = 3


pool_windows = (2, 4, 8, 16)
norm_eps = 1e-06


def padded_2(value, sides, width):
    for axis, dim in sides:
        peers, length = (lax.axis_size(axis), value.shape[dim])
        up = [(i, (i + 1) % peers) for i in range(peers - 1)]
        down = [(j, i) for i, j in up]
        last = lax.slice_in_dim(value, length - width, length, axis=dim)
        initial = lax.slice_in_dim(value, 0, width, axis=dim)
        before = lax.ppermute(last, axis, up)
        after = lax.ppermute(initial, axis, down)
        value = jnp.concatenate([before, value, after], axis=dim)
    return value


def window_means(padded, rows_here, first_row, total_rows, window):
    reach = max(pool_windows) // 2
    half_span = window // 2
    width_cols = padded.shape[1] - 2 * reach
    row_sums = padded[reach - half_span : reach - half_span + rows_here]
    for offset in range(1 - half_span, half_span):
        row_sums = row_sums + padded[reach + offset : reach + offset + rows_here]
    box_sums = row_sums[:, reach - half_span : reach - half_span + width_cols]
    for offset in range(1 - half_span, half_span):
        box_sums = box_sums + row_sums[:, reach + offset : reach + offset + width_cols]
    row_index = first_row + jnp.arange(rows_here, dtype=jnp.int32)
    col_index = jnp.arange(width_cols, dtype=jnp.int32)
    row_counts = jnp.minimum(row_index + half_span, total_rows) - jnp.maximum(
        row_index - half_span, 0
    )
    col_counts = jnp.minimum(col_index + half_span, width_cols) - jnp.maximum(
        col_index - half_span, 0
    )
    counts = (row_counts[:, None] * col_counts[None, :]).astype(jnp.float32)
    return box_sums / counts[:, :, None]


def on_device(tokens_in, norm_gain, w_pool_in, w_gate, w_back):
    reach = max(pool_windows) // 2
    sp_count = lax.axis_size("sp")
    tp_count = lax.axis_size("tp")
    tp_pos = lax.axis_index("tp")
    sp_pos = lax.axis_index("sp")
    tok_rows = tokens_in.shape[0]
    rows_here = tok_rows // GRID_W
    total_rows = rows_here * sp_count
    first_row = sp_pos * rows_here
    local_pool = w_pool_in.shape[2]
    group_width = POOL_WIDTH // GROUPS
    channel_group = (tp_pos * local_pool + jnp.arange(local_pool, dtype=jnp.int32)) // group_width
    state = tokens_in
    for layer_id in range(LAYERS):
        whole_rows = lax.all_gather(state, "tp", axis=1, tiled=True)
        wide = whole_rows.astype(jnp.float32)
        normed = (
            wide
            * lax.rsqrt(jnp.mean(wide * wide, axis=-1, keepdims=True) + norm_eps)
            * norm_gain[layer_id]
        ).astype(jnp.bfloat16)
        pool_acc = jnp.dot(
            normed,
            lax.all_gather(w_pool_in[layer_id], "sp", axis=0, tiled=True),
            preferred_element_type=jnp.float32,
        )
        gate_acc = jnp.dot(
            normed,
            lax.all_gather(w_gate[layer_id], "sp", axis=0, tiled=True),
            preferred_element_type=jnp.float32,
        )
        pool_in = pool_acc.astype(jnp.bfloat16)
        gate = jax.nn.sigmoid(gate_acc)
        cells = pool_in.reshape(rows_here, GRID_W, local_pool)
        rimmed = padded_2(cells, (("sp", 0),), reach)
        padded = jnp.pad(rimmed.astype(jnp.float32), ((0, 0), (reach, reach), (0, 0)))
        means = jnp.zeros((rows_here, GRID_W, local_pool), jnp.float32)
        for group_id in range(GROUPS):
            in_group = (channel_group == group_id)[None, None, :]
            means = jnp.where(
                in_group,
                window_means(padded, rows_here, first_row, total_rows, pool_windows[group_id]),
                means,
            )
        pooled = (
            (means - cells.astype(jnp.float32)).reshape(tok_rows, local_pool).astype(jnp.bfloat16)
        )
        full_pooled = lax.all_gather(pooled, "tp", axis=1, tiled=True)
        back_rows = lax.all_gather(w_back[layer_id], "sp", axis=1, tiled=True)
        back_cols = lax.all_to_all(back_rows, "tp", split_axis=1, concat_axis=0, tiled=True)
        partials = jnp.einsum(
            "tnb,nbd->ntd",
            full_pooled.reshape(tok_rows, tp_count, local_pool),
            back_cols.reshape(tp_count, local_pool, back_cols.shape[1]),
            preferred_element_type=jnp.float32,
        ).astype(jnp.bfloat16)
        branch = jnp.sum(partials.astype(jnp.float32), axis=0)
        state = (state.astype(jnp.float32) + gate * branch).astype(jnp.bfloat16)
    return state


MESH = pl.DeviceIdType.MESH
POOL, GATE, BACK = range(3)


def halves(buffers, layer, block, half):
    views = []
    for buf in buffers:
        rows = buf.shape[2] // 2
        views.append(buf.at[layer, block, pl.ds(pl.multiple_of(half * rows, rows), rows), :])
    return views


def fused_kernel(
    sp_count, tp_count,
    tok_hbm, gain_ref, wp_hbm, wg_hbm, wb_hbm, out_ref,
    wp, wg, wb, gathered, normed, halo, gate_buf, box, counts, parts, arrived,
    load_sem, z_send, z_recv, y_send, y_recv, ag_send, ag_recv, h_send, h_recv, rs_send, rs_recv,
):
    g = lax.axis_index("grp")
    s = lax.axis_index("sp")
    t = lax.axis_index("tp")
    other = 1 - g
    t1 = t + 1 - 2 * (t % 2)
    t2 = (t + 2) % tp_count
    t3 = (t1 + 2) % tp_count
    last = sp_count - 1
    toks, feats = tok_hbm.shape
    rows_here = toks // GRID_W
    total_rows = rows_here * sp_count
    weights = (wp, wg, wb)
    sources = (wp_hbm, wg_hbm, wb_hbm)
    rounds = sp_count - 1

    def load(layer, piece):
        return pltpu.make_async_copy(
            sources[piece].at[layer], weights[piece].at[layer, s], load_sem.at[layer, piece]
        )

    state_load = pltpu.make_async_copy(tok_hbm, gathered.at[0, t], load_sem.at[LAYERS, 0])
    state_load.start()
    for piece in range(3):
        load(0, piece).start()
    for layer in range(1, LAYERS):
        for piece in range(3):
            load(layer, piece).start()

    barrier = pltpu.get_barrier_semaphore()
    for target in ({"grp": other}, {"tp": t1}, {"tp": t2}, {"tp": t3}):
        pl.semaphore_signal(barrier, inc=1, device_id=target, device_id_type=MESH)

    @pl.when(s > 0)
    def _():
        pl.semaphore_signal(barrier, inc=1, device_id={"sp": s - 1}, device_id_type=MESH)

    @pl.when(s < last)
    def _():
        pl.semaphore_signal(barrier, inc=1, device_id={"sp": s + 1}, device_id_type=MESH)

    pl.semaphore_wait(barrier, 4 + jnp.where(s > 0, 1, 0) + jnp.where(s < last, 1, 0))

    def sent_block(way, k):
        return s - k if way == 0 else s + k

    def got_block(way, k):
        return s - 1 - k if way == 0 else s + 1 + k

    def gets(way, k):
        return s - 1 - k >= 0 if way == 0 else s + 1 + k <= last

    def sends(way, k):
        if way == 0:
            return jnp.logical_and(s - k >= 0, s < last)
        return jnp.logical_and(s + k <= last, s > 0)

    def z_copy(layer, way, k, piece, block):
        view = halves(weights, layer, block, g)[piece]
        return pltpu.make_async_remote_copy(
            src_ref=view, dst_ref=view,
            send_sem=z_send.at[layer, way, k, piece], recv_sem=z_recv.at[layer, way, k, piece],
            device_id={"sp": s + 1 if way == 0 else s - 1}, device_id_type=MESH,
        )

    def y_copy(layer, way, k, piece, half):
        view = halves(weights, layer, got_block(way, k), half)[piece]
        return pltpu.make_async_remote_copy(
            src_ref=view, dst_ref=view,
            send_sem=y_send.at[layer, way, k, piece], recv_sem=y_recv.at[layer, way, k, piece],
            device_id={"grp": other}, device_id_type=MESH,
        )

    def own_sends(layer, piece):
        load(layer, piece).wait()
        for way in range(2):
            @pl.when(sends(way, 0))
            def _(way=way):
                z_copy(layer, way, 0, piece, s).start()

    def pump(layer, piece, k):
        for way in range(2):
            @pl.when(gets(way, k))
            def _(way=way):
                z_copy(layer, way, k, piece, got_block(way, k)).wait_recv()
                y_copy(layer, way, k, piece, g).start()
            if k + 1 < rounds:
                @pl.when(sends(way, k + 1))
                def _(way=way):
                    z_copy(layer, way, k + 1, piece, sent_block(way, k + 1)).start()

    def await_y(layer, piece):
        for k in range(rounds):
            for way in range(2):
                @pl.when(gets(way, k))
                def _(way=way, k=k):
                    y_copy(layer, way, k, piece, other).wait_recv()

    def ag_copy(layer, which, block, target):
        return pltpu.make_async_remote_copy(
            src_ref=gathered.at[layer, block], dst_ref=gathered.at[layer, block],
            send_sem=ag_send.at[layer, which], recv_sem=ag_recv.at[layer, which],
            device_id={"tp": target}, device_id_type=MESH,
        )

    def start_gather(layer):
        ag_copy(layer, 0, t, t2).start()
        ag_copy(layer, 1, t, t1).start()

    def h_copy(layer, way):
        return pltpu.make_async_remote_copy(
            src_ref=halo.at[layer, 1], dst_ref=halo.at[layer, 0 if way == 0 else 2],
            send_sem=h_send.at[layer, way], recv_sem=h_recv.at[layer, way],
            device_id={"sp": s + 1 if way == 0 else s - 1}, device_id_type=MESH,
        )

    def rs_copy(layer, which, target):
        return pltpu.make_async_remote_copy(
            src_ref=parts.at[layer, target], dst_ref=arrived.at[layer, which],
            send_sem=rs_send.at[layer, which], recv_sem=rs_recv.at[layer, which],
            device_id={"tp": target}, device_id_type=MESH,
        )

    state_load.wait()
    start_gather(0)
    own_sends(0, POOL)
    own_sends(0, BACK)

    half_span = jnp.int32(pool_windows[0] // 2)
    for group_id in range(1, GROUPS):
        half_span = jnp.where(t == group_id, pool_windows[group_id] // 2, half_span)
    shift = GRID_W.bit_length() - 1
    first_row = s * rows_here
    out_tok = lax.broadcasted_iota(jnp.int32, (toks, toks), 0)
    in_tok = lax.broadcasted_iota(jnp.int32, (toks, toks), 1)
    out_row = first_row + lax.shift_right_logical(out_tok, shift)
    out_col = lax.bitwise_and(out_tok, GRID_W - 1)
    in_col = lax.bitwise_and(in_tok, GRID_W - 1)
    near_col = (in_col >= out_col - half_span) & (in_col < out_col + half_span)
    for slot in range(3):
        in_row = first_row + (slot - 1) * rows_here + lax.shift_right_logical(in_tok, shift)
        inside = (
            near_col
            & (in_row >= out_row - half_span) & (in_row < out_row + half_span)
            & (in_row >= 0) & (in_row < total_rows)
        )
        box[slot] = jnp.where(inside, 1.0, 0.0).astype(jnp.bfloat16)
    tok_at = lax.broadcasted_iota(jnp.int32, counts.shape, 0)
    row_at = first_row + lax.shift_right_logical(tok_at, shift)
    col_at = lax.bitwise_and(tok_at, GRID_W - 1)
    row_counts = jnp.minimum(row_at + half_span, total_rows) - jnp.maximum(row_at - half_span, 0)
    col_counts = jnp.minimum(col_at + half_span, GRID_W) - jnp.maximum(col_at - half_span, 0)
    counts[...] = (row_counts * col_counts).astype(jnp.float32)

    @pl.when(s == 0)
    def _():
        for layer in range(LAYERS):
            halo[layer, 0] = jnp.zeros(halo.shape[2:], halo.dtype)

    @pl.when(s == last)
    def _():
        for layer in range(LAYERS):
            halo[layer, 2] = jnp.zeros(halo.shape[2:], halo.dtype)

    for k in range(rounds):
        pump(0, POOL, k)

    def one_layer(layer, _):
        more = layer + 1 < LAYERS

        pump(layer, BACK, 0)
        own_sends(layer, GATE)
        ag_copy(layer, 0, t2, t2).wait_recv()
        ag_copy(layer, 2, t2, t1).start()
        ag_copy(layer, 1, t1, t1).wait_recv()
        ag_copy(layer, 2, t3, t1).wait_recv()
        total = jnp.zeros((toks, 1), jnp.float32)
        for block in range(tp_count):
            wide = gathered[layer, block].astype(jnp.float32)
            total = total + jnp.sum(wide * wide, axis=1, keepdims=True)
        scale = lax.rsqrt(total / (tp_count * feats) + norm_eps)
        for block in range(tp_count):
            cols = slice(block * feats, (block + 1) * feats)
            wide = gathered[layer, block].astype(jnp.float32)
            normed[:, cols] = (wide * scale * gain_ref[pl.ds(layer, 1), cols]).astype(jnp.bfloat16)

        for k in range(1, rounds - 1):
            pump(layer, BACK, k)
        depth = wp.shape[2]

        def project(buf):
            acc = None
            for block in range(sp_count):
                term = jnp.dot(
                    normed[:, block * depth:(block + 1) * depth], buf[layer, block],
                    preferred_element_type=jnp.float32,
                )
                acc = term if acc is None else acc + term
            return acc

        await_y(layer, POOL)
        halo[layer, 1] = project(wp).astype(jnp.bfloat16)

        @pl.when(s < last)
        def _():
            h_copy(layer, 0).start()

        @pl.when(s > 0)
        def _():
            h_copy(layer, 1).start()

        pump(layer, BACK, rounds - 1)

        pump(layer, GATE, 0)

        @pl.when(more)
        def _():
            own_sends(layer + 1, POOL)


        @pl.when(s > 0)
        def _():
            h_copy(layer, 0).wait_recv()

        @pl.when(s < last)
        def _():
            h_copy(layer, 1).wait_recv()

        sums = jnp.zeros(counts.shape, jnp.float32)
        for slot in range(3):
            sums = sums + jnp.dot(box[slot], halo[layer, slot], preferred_element_type=jnp.float32)
        pooled = (sums / counts[...] - halo[layer, 1].astype(jnp.float32)).astype(jnp.bfloat16)
        await_y(layer, BACK)
        for which, target in ((1, t3), (0, t2), (2, t1), (None, t)):
            parts[layer, target] = jnp.dot(
                pooled, wb[layer, target], preferred_element_type=jnp.float32
            ).astype(jnp.bfloat16)
            if which is not None:
                rs_copy(layer, which, target).start()

        for k in range(1, rounds):
            pump(layer, GATE, k)

        @pl.when(more)
        def _():
            pump(layer + 1, POOL, 0)
            own_sends(layer + 1, BACK)
            for k in range(1, rounds - 1):
                pump(layer + 1, POOL, k)

        await_y(layer, GATE)
        gate_buf[...] = jax.nn.sigmoid(project(wg))
        branch = parts[layer, t].astype(jnp.float32)
        for which in (2, 0, 1):
            rs_copy(layer, which, t1).wait_recv()
            branch = branch + arrived[layer, which].astype(jnp.float32)
        state = (gathered[layer, t].astype(jnp.float32) + gate_buf[...] * branch).astype(jnp.bfloat16)

        @pl.when(more)
        def _():
            gathered[layer + 1, t] = state
            start_gather(layer + 1)
            pump(layer + 1, POOL, rounds - 1)

        @pl.when(layer + 1 == LAYERS)
        def _():
            out_ref[...] = state

        return 0

    lax.fori_loop(0, LAYERS, one_layer, 0)

    def drain(layer, _):
        for piece in range(3):
            for k in range(rounds):
                for way in range(2):
                    @pl.when(sends(way, k))
                    def _(way=way, k=k, piece=piece):
                        z_copy(layer, way, k, piece, sent_block(way, k)).wait_send()

                    @pl.when(gets(way, k))
                    def _(way=way, k=k, piece=piece):
                        y_copy(layer, way, k, piece, g).wait_send()
        ag_copy(layer, 0, t, t2).wait_send()
        ag_copy(layer, 1, t, t1).wait_send()
        ag_copy(layer, 2, t2, t1).wait_send()

        @pl.when(s < last)
        def _():
            h_copy(layer, 0).wait_send()

        @pl.when(s > 0)
        def _():
            h_copy(layer, 1).wait_send()

        rs_copy(layer, 0, t2).wait_send()
        rs_copy(layer, 1, t3).wait_send()
        rs_copy(layer, 2, t1).wait_send()
        return 0

    lax.fori_loop(0, LAYERS, drain, 0)


def fused(tokens_in, norm_gain, w_pool_in, w_gate, w_back):
    sp_count, tp_count = lax.axis_size("sp"), lax.axis_size("tp")
    toks, feats = tokens_in.shape
    _, depth, local_pool = w_pool_in.shape
    rounds = sp_count - 1
    bf, f32 = jnp.bfloat16, jnp.float32
    dma = pltpu.SemaphoreType.DMA
    streams = dma((LAYERS, 2, rounds, 3))
    return pl.pallas_call(
        functools.partial(fused_kernel, sp_count, tp_count),
        out_shape=jax.ShapeDtypeStruct((toks, feats), bf),
        in_specs=[
            pl.BlockSpec(memory_space=pltpu.HBM),
            pl.BlockSpec(memory_space=pltpu.VMEM),
            pl.BlockSpec(memory_space=pltpu.HBM),
            pl.BlockSpec(memory_space=pltpu.HBM),
            pl.BlockSpec(memory_space=pltpu.HBM),
        ],
        out_specs=pl.BlockSpec(memory_space=pltpu.VMEM),
        scratch_shapes=[
            pltpu.VMEM((LAYERS, sp_count) + w_pool_in.shape[1:], bf),
            pltpu.VMEM((LAYERS, sp_count) + w_gate.shape[1:], bf),
            pltpu.VMEM((LAYERS, sp_count) + w_back.shape[1:], bf),
            pltpu.VMEM((LAYERS, tp_count, toks, feats), bf),
            pltpu.VMEM((toks, tp_count * feats), bf),
            pltpu.VMEM((LAYERS, 3, toks, local_pool), bf),
            pltpu.VMEM((toks, feats), f32),
            pltpu.VMEM((3, toks, toks), bf),
            pltpu.VMEM((toks, local_pool), f32),
            pltpu.VMEM((LAYERS, tp_count, toks, feats), bf),
            pltpu.VMEM((LAYERS, 3, toks, feats), bf),
            dma((LAYERS + 1, 3)),
            streams, streams, streams, streams,
            dma((LAYERS, 3)), dma((LAYERS, 3)),
            dma((LAYERS, 2)), dma((LAYERS, 2)),
            dma((LAYERS, 3)), dma((LAYERS, 3)),
        ],
        compiler_params=pltpu.CompilerParams(
            collective_id=0, has_side_effects=True, vmem_limit_bytes=56 * 1024 * 1024
        ),
    )(tokens_in, norm_gain, w_pool_in, w_gate, w_back)


def dispatch(tokens_in, norm_gain, w_pool_in, w_gate, w_back):
    fits = (
        lax.axis_size("grp") == 2
        and lax.axis_size("tp") == GROUPS == 4
        and lax.axis_size("sp") == lax.axis_size("tp")
        and w_pool_in.shape[2] * GROUPS == POOL_WIDTH
        and w_pool_in.shape[1] == tokens_in.shape[1]
        and tokens_in.shape[0] // GRID_W >= max(pool_windows) // 2
    )
    step = fused if fits else on_device
    return step(tokens_in, norm_gain, w_pool_in, w_gate, w_back)


def solution(mesh):
    return jax.shard_map(
        dispatch,
        mesh=mesh,
        in_specs=(
            P(("grp", "sp"), "tp"),
            P(),
            P(None, "sp", "tp"),
            P(None, "sp", "tp"),
            P(None, "tp", "sp"),
        ),
        out_specs=P(("grp", "sp"), "tp"),
        check_vma=False,
    )
```

profile of v0, /device:TPU:0, one launch (start us, length us, event | category | flops | bytes accessed | tf_op | source)
XLA Modules:
  0.0 130.9 jit_solution(12084254394706787641)
XLA Ops:
  0.0 129.2 %shard_map.55 = bf16[256,512]{1,0:T(8,128)(2,1)} custom-call(bf16[256,512]{1,0:T(8,128)(2,1)} %tok_hbm.1, f32[3,2048]{1,0:T(4,128)} %gain_ref.1, bf16[3,512,256]{2,1,0:T(8,128)(2,1)} %wp_hbm.1, bf16[3,512,512]{2,1,0:T(8,128)(2,1)} %wg_hbm.1, bf16[3,256,512]{2,1,0:T(8,128)(2,1)} %wb_hbm.1), custom_call_target="tpu_custom_call" | custom-call | tf_op jit(solution)/shard_map/pallas_call | solution.py:444
  129.2 1.7 %copy.7 = bf16[256,512]{1,0:T(8,128)(2,1)} copy(bf16[256,512]{1,0:T(8,128)(2,1)} %shard_map.55) | data formatting | bytes 524288
where the time goes:
time: 131 us
  Pallas kernels  129 us (98%)
  local copies, waits for them, and re-layouts  1.67 us (1%)
    pallas_call x1, Pallas kernels, fused(): pl.pallas_call(functools.partial(fused_kernel, sp_count, tp_count), out_s...  129 us

commit v1 on v0

v1 whole, which is shorter than its diff:
```python
import jax
import jax.numpy as jnp
from jax import lax
from jax.experimental import pallas as pl
from jax.experimental.pallas import tpu as pltpu
from jax.sharding import PartitionSpec as P
import functools

POOL_WIDTH = 1024
GROUPS = 4
GRID_W = 32
LAYERS = 3


pool_windows = (2, 4, 8, 16)
norm_eps = 1e-06


def padded_2(value, sides, width):
    for axis, dim in sides:
        peers, length = (lax.axis_size(axis), value.shape[dim])
        up = [(i, (i + 1) % peers) for i in range(peers - 1)]
        down = [(j, i) for i, j in up]
        last = lax.slice_in_dim(value, length - width, length, axis=dim)
        initial = lax.slice_in_dim(value, 0, width, axis=dim)
        before = lax.ppermute(last, axis, up)
        after = lax.ppermute(initial, axis, down)
        value = jnp.concatenate([before, value, after], axis=dim)
    return value


def window_means(padded, rows_here, first_row, total_rows, window):
    reach = max(pool_windows) // 2
    half_span = window // 2
    width_cols = padded.shape[1] - 2 * reach
    row_sums = padded[reach - half_span : reach - half_span + rows_here]
    for offset in range(1 - half_span, half_span):
        row_sums = row_sums + padded[reach + offset : reach + offset + rows_here]
    box_sums = row_sums[:, reach - half_span : reach - half_span + width_cols]
    for offset in range(1 - half_span, half_span):
        box_sums = box_sums + row_sums[:, reach + offset : reach + offset + width_cols]
    row_index = first_row + jnp.arange(rows_here, dtype=jnp.int32)
    col_index = jnp.arange(width_cols, dtype=jnp.int32)
    row_counts = jnp.minimum(row_index + half_span, total_rows) - jnp.maximum(
        row_index - half_span, 0
    )
    col_counts = jnp.minimum(col_index + half_span, width_cols) - jnp.maximum(
        col_index - half_span, 0
    )
    counts = (row_counts[:, None] * col_counts[None, :]).astype(jnp.float32)
    return box_sums / counts[:, :, None]


def on_device(tokens_in, norm_gain, w_pool_in, w_gate, w_back):
    reach = max(pool_windows) // 2
    sp_count = lax.axis_size("sp")
    tp_count = lax.axis_size("tp")
    tp_pos = lax.axis_index("tp")
    sp_pos = lax.axis_index("sp")
    tok_rows = tokens_in.shape[0]
    rows_here = tok_rows // GRID_W
    total_rows = rows_here * sp_count
    first_row = sp_pos * rows_here
    local_pool = w_pool_in.shape[2]
    group_width = POOL_WIDTH // GROUPS
    channel_group = (tp_pos * local_pool + jnp.arange(local_pool, dtype=jnp.int32)) // group_width
    state = tokens_in
    for layer_id in range(LAYERS):
        whole_rows = lax.all_gather(state, "tp", axis=1, tiled=True)
        wide = whole_rows.astype(jnp.float32)
        normed = (
            wide
            * lax.rsqrt(jnp.mean(wide * wide, axis=-1, keepdims=True) + norm_eps)
            * norm_gain[layer_id]
        ).astype(jnp.bfloat16)
        pool_acc = jnp.dot(
            normed,
            lax.all_gather(w_pool_in[layer_id], "sp", axis=0, tiled=True),
            preferred_element_type=jnp.float32,
        )
        gate_acc = jnp.dot(
            normed,
            lax.all_gather(w_gate[layer_id], "sp", axis=0, tiled=True),
            preferred_element_type=jnp.float32,
        )
        pool_in = pool_acc.astype(jnp.bfloat16)
        gate = jax.nn.sigmoid(gate_acc)
        cells = pool_in.reshape(rows_here, GRID_W, local_pool)
        rimmed = padded_2(cells, (("sp", 0),), reach)
        padded = jnp.pad(rimmed.astype(jnp.float32), ((0, 0), (reach, reach), (0, 0)))
        means = jnp.zeros((rows_here, GRID_W, local_pool), jnp.float32)
        for group_id in range(GROUPS):
            in_group = (channel_group == group_id)[None, None, :]
            means = jnp.where(
                in_group,
                window_means(padded, rows_here, first_row, total_rows, pool_windows[group_id]),
                means,
            )
        pooled = (
            (means - cells.astype(jnp.float32)).reshape(tok_rows, local_pool).astype(jnp.bfloat16)
        )
        full_pooled = lax.all_gather(pooled, "tp", axis=1, tiled=True)
        back_rows = lax.all_gather(w_back[layer_id], "sp", axis=1, tiled=True)
        back_cols = lax.all_to_all(back_rows, "tp", split_axis=1, concat_axis=0, tiled=True)
        partials = jnp.einsum(
            "tnb,nbd->ntd",
            full_pooled.reshape(tok_rows, tp_count, local_pool),
            back_cols.reshape(tp_count, local_pool, back_cols.shape[1]),
            preferred_element_type=jnp.float32,
        ).astype(jnp.bfloat16)
        branch = jnp.sum(partials.astype(jnp.float32), axis=0)
        state = (state.astype(jnp.float32) + gate * branch).astype(jnp.bfloat16)
    return state


MESH = pl.DeviceIdType.MESH
POOL, GATE_A, GATE_B, BACK = range(4)
UNITS = {POOL: (0,), GATE_A: (1,), GATE_B: (2,), BACK: (3, 4)}
CHUNKS = 2
GUEST = LAYERS


def fused_kernel(
    sp_count, tp_count,
    tok_hbm, gain_ref, wp_hbm, wg_hbm, wb_hbm, out_ref,
    wp, wg, wb, wb_own, gathered, scaled, halo, gate_buf, own_part, box, counts,
    pair, parts, arrived, returned,
    load_sem, w_send, w_recv, bx_send, bx_recv, tk_send, tk_recv, rt_send, rt_recv,
    ag_send, ag_recv, h_send, h_recv, px_send, px_recv, rs_send, rs_recv,
):
    g = lax.axis_index("grp")
    s = lax.axis_index("sp")
    t = lax.axis_index("tp")
    other = 1 - g
    c = t % 2
    base = t - c
    t1 = base + 1 - c
    t2 = (t + 2) % tp_count
    t3 = (t1 + 2) % tp_count
    far_base = (base + 2) % tp_count
    last = sp_count - 1
    toks, feats = tok_hbm.shape
    local_pool = wp.shape[2]
    cols_k = feats // CHUNKS
    rows_here = toks // GRID_W
    total_rows = rows_here * sp_count
    bf, f32 = jnp.bfloat16, jnp.float32

    low = s < 2
    is_mid = jnp.logical_and(s > 0, s < last)
    is_end = jnp.logical_not(is_mid)
    end_here = jnp.where(low, 0, last)
    mid_here = jnp.where(low, 1, last - 1)
    end_far = last - end_here
    mid_far = last - mid_here
    blocks = (
        jnp.where(is_mid, end_here, mid_here),
        jnp.where(is_mid, mid_far, mid_far),
        end_far,
    )
    s_parity = s % 2

    p_rows, g_rows = wp_hbm.shape[1], wg_hbm.shape[1]
    b_rows = wb_hbm.shape[1]

    def view(layer, block, half, unit, row=None):
        if unit == 0:
            n = p_rows // 2
            return wp.at[layer, pl.ds(pl.multiple_of(block * p_rows + half * n, n), n), :]
        if unit in (1, 2):
            n = g_rows // 4
            at = block * g_rows + half * (2 * n) + (unit - 1) * n
            return wg.at[layer, pl.ds(pl.multiple_of(at, n), n), :]
        n = b_rows // 2
        row = unit - 3 if row is None else row
        return wb.at[layer, block // 2, pl.ds(pl.multiple_of(row * b_rows + half * n, n), n), :]

    def w_copy(layer, flow, block, half, unit, target):
        ref = view(layer, block, half, unit)
        return pltpu.make_async_remote_copy(
            src_ref=ref, dst_ref=ref,
            send_sem=w_send.at[layer, flow, unit], recv_sem=w_recv.at[layer, block, half, unit],
            device_id=target, device_id_type=MESH,
        )

    def own_copy(layer, flow, half, piece, plane):
        if piece != BACK:
            return w_copy(layer, flow, s, half, UNITS[piece][0], {"sp": plane})
        n = b_rows // 2
        return pltpu.make_async_remote_copy(
            src_ref=wb_own.at[layer, pl.ds(pl.multiple_of(half * n, n), n), :],
            dst_ref=view(layer, s, half, 3, row=c),
            send_sem=w_send.at[layer, flow, 3], recv_sem=w_recv.at[layer, s, half, 3 + c],
            device_id={"sp": plane, "tp": base + s_parity}, device_id_type=MESH,
        )

    def near_copy(layer, block, unit):
        target = {"grp": jnp.where(is_mid, g, other), "sp": jnp.where(is_mid, mid_far, s)}
        return w_copy(layer, 2, block, g, unit, target)

    def across_copy(layer, k, block, unit):
        return w_copy(layer, 2 + k, block, g, unit, {"grp": other})

    def outer_copy(layer, k, block, unit):
        return w_copy(layer, 4 + k, block, g, unit, {"sp": end_here})

    def holds(block, piece, fn):
        if piece == BACK:
            pl.when(c == block % 2)(fn)
        else:
            fn()

    def pump(layer, k, *pieces):
        block = blocks[k]
        for piece in pieces:
            def act(piece=piece):
                for unit in UNITS[piece]:
                    w_copy(layer, 0, block, g, unit, {"grp": other}).wait_recv()
                    if k == 0:
                        near_copy(layer, block, unit).start()
                    else:
                        across_copy(layer, k, block, unit).start()

                        @pl.when(jnp.logical_and(is_mid, layer > 0))
                        def _(unit=unit):
                            outer_copy(layer, k, block, unit).start()
            holds(block, piece, act)

    def bx_copy(layer):
        return pltpu.make_async_remote_copy(
            src_ref=wb_own.at[layer],
            dst_ref=wb.at[layer, s // 2, pl.ds(pl.multiple_of(c * b_rows, b_rows), b_rows), :],
            send_sem=bx_send.at[layer], recv_sem=bx_recv.at[layer],
            device_id={"tp": t1}, device_id_type=MESH,
        )

    def wb_load(layer):
        return pltpu.make_async_copy(
            wb_hbm.at[layer],
            wb.at[layer, s // 2, pl.ds(pl.multiple_of(c * b_rows, b_rows), b_rows), :],
            load_sem.at[layer, 3],
        )

    def load(layer, piece):
        if piece == 0:
            src, dst = wp_hbm.at[layer], wp.at[layer, pl.ds(pl.multiple_of(s * p_rows, p_rows), p_rows), :]
        elif piece == 1:
            src, dst = wg_hbm.at[layer], wg.at[layer, pl.ds(pl.multiple_of(s * g_rows, g_rows), g_rows), :]
        else:
            src, dst = wb_hbm.at[layer], wb_own.at[layer]
        return pltpu.make_async_copy(src, dst, load_sem.at[layer, piece])

    def ready(layer, *pieces):
        for piece in pieces:
            for k in range(3):
                block = blocks[k]

                def act(piece=piece, block=block):
                    for unit in UNITS[piece]:
                        w_copy(layer, 0, block, other, unit, {"grp": other}).wait_recv()
                holds(block, piece, act)
            if piece == BACK:
                @pl.when(c == s_parity)
                def _():
                    wb_load(layer).wait()
                    pltpu.make_async_remote_copy(
                        src_ref=wb_own.at[layer],
                        dst_ref=wb.at[layer, s // 2, pl.ds(pl.multiple_of((1 - c) * b_rows, b_rows), b_rows), :],
                        send_sem=bx_send.at[layer], recv_sem=bx_recv.at[layer],
                        device_id={"tp": t1}, device_id_type=MESH,
                    ).wait_recv()

    def tok_load(k):
        return pltpu.make_async_copy(
            tok_hbm.at[:, pl.ds(k * cols_k, cols_k)], gathered.at[0, t, k], load_sem.at[LAYERS, k]
        )

    def guest_copy(k):
        return pltpu.make_async_remote_copy(
            src_ref=gathered.at[0, t, k], dst_ref=gathered.at[GUEST, t, k],
            send_sem=tk_send.at[k], recv_sem=tk_recv.at[k],
            device_id={"sp": mid_here}, device_id_type=MESH,
        )

    def return_copy(k):
        return pltpu.make_async_remote_copy(
            src_ref=returned.at[k], dst_ref=gathered.at[1, t, k],
            send_sem=rt_send.at[k], recv_sem=rt_recv.at[k],
            device_id={"sp": end_here}, device_id_type=MESH,
        )

    def ag_copy(slot, which, k, block, target):
        return pltpu.make_async_remote_copy(
            src_ref=gathered.at[slot, block, k], dst_ref=gathered.at[slot, block, k],
            send_sem=ag_send.at[slot, which, k], recv_sem=ag_recv.at[slot, which, k],
            device_id={"tp": target}, device_id_type=MESH,
        )

    def start_gather(slot, k):
        ag_copy(slot, 0, k, t, t2).start()
        ag_copy(slot, 1, k, t, t1).start()

    spans = [w // 2 for w in pool_windows]

    def h_copy(layer, way, span):
        rows = (span if way == 0 else max(span - 1, 1)) * GRID_W
        at = toks - rows if way == 0 else 0
        return pltpu.make_async_remote_copy(
            src_ref=halo.at[layer, 1, pl.ds(at, rows), :],
            dst_ref=halo.at[layer, 0 if way == 0 else 2, pl.ds(at, rows), :],
            send_sem=h_send.at[layer, way], recv_sem=h_recv.at[layer, way],
            device_id={"sp": s + 1 if way == 0 else s - 1}, device_id_type=MESH,
        )

    def halo_do(layer, way, cond, op):
        for group_id, span in enumerate(spans):
            @pl.when(jnp.logical_and(cond, t == group_id))
            def _(span=span):
                op(h_copy(layer, way, span))

    def halo_start(layer):
        up_ok = jnp.logical_and(s < last, jnp.logical_or(layer > 0, s == 1))
        down_ok = jnp.logical_and(s > 0, jnp.logical_or(layer > 0, s == 2))
        halo_do(layer, 0, up_ok, lambda x: x.start())
        halo_do(layer, 1, down_ok, lambda x: x.start())

    def halo_wait(layer):
        from_up = jnp.logical_and(s > 0, jnp.logical_or(layer > 0, s == 2))
        from_down = jnp.logical_and(s < last, jnp.logical_or(layer > 0, s == 1))
        halo_do(layer, 0, from_up, lambda x: x.wait_recv())
        halo_do(layer, 1, from_down, lambda x: x.wait_recv())

    def px_copy(slot, row):
        return pltpu.make_async_remote_copy(
            src_ref=pair.at[slot, row], dst_ref=pair.at[slot, row],
            send_sem=px_send.at[slot], recv_sem=px_recv.at[slot],
            device_id={"tp": t1}, device_id_type=MESH,
        )

    def rs_copy(slot, k):
        return pltpu.make_async_remote_copy(
            src_ref=parts.at[slot, k], dst_ref=arrived.at[slot, k],
            send_sem=rs_send.at[slot, k], recv_sem=rs_recv.at[slot, k],
            device_id={"tp": t2}, device_id_type=MESH,
        )

    def absorb(layer, slot, which, block, total):
        for k in range(CHUNKS):
            at = pl.ds(pl.multiple_of(block * feats + k * cols_k, cols_k), cols_k)
            wide = gathered[slot, block, k].astype(f32)
            scaled[which, :, at] = (wide * gain_ref[pl.ds(layer, 1), at]).astype(bf)
            total = total + jnp.sum(wide * wide, axis=1, keepdims=True)
        return total

    def scale_of(total):
        return lax.rsqrt(total / (tp_count * feats) + norm_eps)

    def half_dot(layer, which, first, weights):
        at = pl.ds(pl.multiple_of(first * feats, feats), 2 * feats)
        return jnp.dot(scaled[which, :, at], weights[layer, at, :], preferred_element_type=f32)

    def gate_of(layer, which, scale):
        acc = jnp.dot(scaled[which], wg[layer], preferred_element_type=f32)
        value = jax.nn.sigmoid(acc * scale)
        for k in range(CHUNKS):
            gate_buf[which, k] = value[:, k * cols_k:(k + 1) * cols_k]

    def share_pooled(slot, which, sums, cells):
        pooled = (sums / counts[which] - cells.astype(f32)).astype(bf)
        pair[slot, c] = pooled
        px_copy(slot, c).start()

    def back_part(layer, slot, cols, k):
        at = pl.ds(k * cols_k, cols_k)
        acc = jnp.dot(pair[slot, 0], wb[layer, cols, 0:b_rows, at], preferred_element_type=f32)
        return acc + jnp.dot(
            pair[slot, 1], wb[layer, cols, b_rows:2 * b_rows, at], preferred_element_type=f32
        )

    def back(layer, slot, which):
        px_copy(slot, 1 - c).wait_recv()
        for k in range(CHUNKS):
            parts[slot, k] = back_part(layer, slot, far_base // 2, k).astype(bf)
            rs_copy(slot, k).start()
        for k in range(CHUNKS):
            own_part[which, k] = back_part(layer, slot, base // 2, k)

    def update(slot, which, k):
        rs_copy(slot, k).wait_recv()
        branch = own_part[which, k] + arrived[slot, k].astype(f32)
        return (gathered[slot, t, k].astype(f32) + gate_buf[which, k] * branch).astype(bf)

    for k in range(CHUNKS):
        tok_load(k).start()
    for layer in range(LAYERS):
        for piece in (0, 2, 1):
            load(layer, piece).start()

        @pl.when(jnp.logical_and(c == s_parity, jnp.logical_or(is_mid, layer > 0)))
        def _(layer=layer):
            wb_load(layer).start()
    for layer in range(LAYERS):
        for slot in (0, 2):
            halo[layer, slot] = jnp.zeros(halo.shape[2:], halo.dtype)

    barrier = pltpu.get_barrier_semaphore()
    for target in ({"grp": other}, {"tp": t1}, {"tp": t2}):
        pl.semaphore_signal(barrier, inc=1, device_id=target, device_id_type=MESH)

    @pl.when(s > 0)
    def _():
        for peer in (t, t1):
            pl.semaphore_signal(barrier, inc=1, device_id={"sp": s - 1, "tp": peer}, device_id_type=MESH)

    @pl.when(s < last)
    def _():
        for peer in (t, t1):
            pl.semaphore_signal(barrier, inc=1, device_id={"sp": s + 1, "tp": peer}, device_id_type=MESH)

    pl.semaphore_wait(barrier, 3 + jnp.where(s > 0, 2, 0) + jnp.where(s < last, 2, 0))

    def own_loads(layer):
        for piece in (0, 2, 1):
            load(layer, piece).wait()

        @pl.when(c != s_parity)
        def _():
            bx_copy(layer).start()

    PIECES = (POOL, BACK, GATE_A, GATE_B)

    def end_own(layer, mine, *pieces):
        for piece in pieces:
            half = g if mine else other
            own_copy(layer, 0 if mine else 1, half, piece, mid_here).start()

    def mid_own(layer, flow, *pieces):
        plane = mid_far if flow == 0 else end_here
        for piece in pieces:
            own_copy(layer, flow, g, piece, plane).start()

    def setup():
        half_span = jnp.int32(spans[0])
        for group_id in range(1, GROUPS):
            half_span = jnp.where(t == group_id, spans[group_id], half_span)
        shift = GRID_W.bit_length() - 1
        out_tok = lax.broadcasted_iota(jnp.int32, (toks, toks), 0)
        in_tok = lax.broadcasted_iota(jnp.int32, (toks, toks), 1)
        out_row = lax.shift_right_logical(out_tok, shift)
        out_col = lax.bitwise_and(out_tok, GRID_W - 1)
        in_col = lax.bitwise_and(in_tok, GRID_W - 1)
        near_col = (in_col >= out_col - half_span) & (in_col < out_col + half_span)
        for slot in range(3):
            in_row = (slot - 1) * rows_here + lax.shift_right_logical(in_tok, shift)
            inside = near_col & (in_row >= out_row - half_span) & (in_row < out_row + half_span)
            box[slot] = jnp.where(inside, 1.0, 0.0).astype(bf)
        tok_at = lax.broadcasted_iota(jnp.int32, counts.shape[1:], 0)
        col_at = lax.bitwise_and(tok_at, GRID_W - 1)
        col_counts = jnp.minimum(col_at + half_span, GRID_W) - jnp.maximum(col_at - half_span, 0)
        for which, plane in ((0, s), (1, end_here)):
            row_at = plane * rows_here + lax.shift_right_logical(tok_at, shift)
            row_counts = jnp.minimum(row_at + half_span, total_rows) - jnp.maximum(row_at - half_span, 0)
            counts[which] = (row_counts * col_counts).astype(f32)

    def box_dot(slot, value):
        return jnp.dot(box[slot], value, preferred_element_type=f32)

    for k in range(CHUNKS):
        tok_load(k).wait()

    @pl.when(is_end)
    def _():
        load(0, 0).wait()
        end_own(0, True, POOL)
        for k in range(CHUNKS):
            guest_copy(k).start()
        end_own(0, False, POOL)
        load(0, 2).wait()
        end_own(0, True, BACK)
        load(0, 1).wait()
        end_own(0, True, GATE_A, GATE_B)
        end_own(0, False, BACK, GATE_A, GATE_B)
        own_loads(1)
        own_loads(2)
        setup()
        pump(1, 0, POOL, BACK, GATE_A, GATE_B)
        pump(2, 0, POOL)
        end_own(1, True, POOL, BACK)
        pump(2, 0, BACK, GATE_A, GATE_B)
        end_own(1, True, GATE_A, GATE_B)
        end_own(1, False, POOL, BACK)
        for k in range(CHUNKS):
            return_copy(k).wait_recv()
            start_gather(1, k)
        pump(1, 1, POOL)

    @pl.when(is_mid)
    def _():
        guest_side = jnp.where(low, 0, 2)
        for k in range(CHUNKS):
            start_gather(0, k)
        load(0, 0).wait()
        mid_own(0, 0, POOL)
        load(0, 2).wait()
        mid_own(0, 0, BACK)
        load(0, 1).wait()
        mid_own(0, 0, GATE_A, GATE_B)

        @pl.when(c != s_parity)
        def _():
            bx_copy(0).start()
        own_loads(1)
        own_loads(2)
        mid_own(1, 1, *PIECES)
        mid_own(2, 1, *PIECES)
        zero = jnp.zeros((toks, 1), f32)
        total = absorb(0, 0, 0, t, zero)
        pump(0, 1, POOL)
        pump(0, 0, POOL)
        setup()
        for k in range(CHUNKS):
            guest_copy(k).wait_recv()
            start_gather(GUEST, k)
        for k in range(CHUNKS):
            ag_copy(0, 1, k, t1, t1).wait_recv()
            ag_copy(0, 0, k, t2, t2).wait_recv()
            ag_copy(0, 2, k, t2, t1).start()
        total = absorb(0, 0, 0, t1, total)
        pump(0, 1, BACK)
        pump(0, 2, POOL)
        total = absorb(0, 0, 0, t2, total)
        for k in range(CHUNKS):
            ag_copy(0, 2, k, t3, t1).wait_recv()
        total = absorb(0, 0, 0, t3, total)
        scale = scale_of(total)
        guest_total = absorb(0, GUEST, 1, t, zero)
        pump(0, 1, GATE_A)
        for k in range(CHUNKS):
            ag_copy(GUEST, 1, k, t1, t1).wait_recv()
            ag_copy(GUEST, 0, k, t2, t2).wait_recv()
            ag_copy(GUEST, 2, k, t2, t1).start()
        pump(0, 0, BACK)
        guest_total = absorb(0, GUEST, 1, t1, guest_total)
        guest_total = absorb(0, GUEST, 1, t2, guest_total)
        ready(0, POOL)
        acc = half_dot(0, 0, base, wp) + half_dot(0, 0, far_base, wp)
        halo[0, 1] = (acc * scale).astype(bf)
        halo_start(0)
        for k in range(CHUNKS):
            ag_copy(GUEST, 2, k, t3, t1).wait_recv()
        guest_total = absorb(0, GUEST, 1, t3, guest_total)
        guest_scale = scale_of(guest_total)
        acc = half_dot(0, 1, base, wp) + half_dot(0, 1, far_base, wp)
        halo[0, guest_side] = (acc * guest_scale).astype(bf)
        cells = halo[0, guest_side]
        own_cells = halo[0, 1]
        share_pooled(GUEST, 1, box_dot(1, cells) + box_dot(2 - guest_side, own_cells), cells)
        pump(0, 1, GATE_B)
        pump(0, 0, GATE_A)
        pump(0, 2, BACK)
        halo_wait(0)
        sums = box_dot(0, halo[0, 0]) + box_dot(1, own_cells) + box_dot(2, halo[0, 2])
        share_pooled(0, 0, sums, own_cells)
        pump(0, 0, GATE_B)
        mid_own(1, 0, *PIECES)
        ready(0, BACK)
        back(0, GUEST, 1)
        back(0, 0, 0)
        pump(0, 2, GATE_A, GATE_B)
        ready(0, GATE_A, GATE_B)
        gate_of(0, 1, guest_scale)
        for k in range(CHUNKS):
            returned[k] = update(GUEST, 1, k)
            return_copy(k).start()
        gate_of(0, 0, scale)
        for k in range(CHUNKS):
            gathered[1, t, k] = update(0, 0, k)
            start_gather(1, k)
        pump(1, 1, POOL)

    def one_layer(layer, _):
        more = layer + 1 < LAYERS
        @pl.when(jnp.logical_and(is_mid, layer == 1))
        def _():
            pump(layer, 0, POOL)
        pump(layer, 2, POOL)
        total = absorb(layer, layer, 0, t, jnp.zeros((toks, 1), f32))
        pump(layer, 1, BACK)
        for k in range(CHUNKS):
            ag_copy(layer, 1, k, t1, t1).wait_recv()
        total = absorb(layer, layer, 0, t1, total)
        for k in range(CHUNKS):
            ag_copy(layer, 0, k, t2, t2).wait_recv()
            ag_copy(layer, 2, k, t2, t1).start()
        total = absorb(layer, layer, 0, t2, total)
        ready(layer, POOL)
        acc = half_dot(layer, 0, base, wp)
        for k in range(CHUNKS):
            ag_copy(layer, 2, k, t3, t1).wait_recv()
        total = absorb(layer, layer, 0, t3, total)
        scale = scale_of(total)
        acc = acc + half_dot(layer, 0, far_base, wp)
        halo[layer, 1] = (acc * scale).astype(bf)
        halo_start(layer)

        @pl.when(is_end)
        def _():
            end_own(layer, False, GATE_A, GATE_B)

            @pl.when(more)
            def _():
                end_own(layer + 1, True, POOL, BACK)
                end_own(layer + 1, False, POOL, BACK)
                end_own(layer + 1, True, GATE_A, GATE_B)

        @pl.when(is_mid)
        def _():
            pump(layer, 0, BACK)
        pump(layer, 2, BACK)

        @pl.when(is_mid)
        def _():
            pump(layer, 0, GATE_A)
        pump(layer, 1, GATE_A)
        cells = halo[layer, 1]
        sums = box_dot(1, cells)
        halo_wait(layer)
        sums = sums + box_dot(0, halo[layer, 0]) + box_dot(2, halo[layer, 2])
        share_pooled(layer, 0, sums, cells)

        @pl.when(is_mid)
        def _():
            pump(layer, 0, GATE_B)
        pump(layer, 1, GATE_B)

        @pl.when(jnp.logical_and(is_mid, more))
        def _():
            mid_own(layer + 1, 0, *PIECES)
        ready(layer, BACK)
        back(layer, layer, 0)
        pump(layer, 2, GATE_A, GATE_B)

        @pl.when(more)
        def _():
            pump(layer + 1, 1, POOL)

            @pl.when(is_mid)
            def _():
                pump(layer + 1, 0, POOL)
        ready(layer, GATE_A, GATE_B)
        gate_of(layer, 0, scale)
        for k in range(CHUNKS):
            state = update(layer, 0, k)

            @pl.when(more)
            def _(k=k, state=state):
                gathered[layer + 1, t, k] = state
                start_gather(layer + 1, k)

            @pl.when(jnp.logical_not(more))
            def _(k=k, state=state):
                out_ref[:, k * cols_k:(k + 1) * cols_k] = state
        return 0

    lax.fori_loop(1, LAYERS, one_layer, 0)

    def drain_own(layer, flow, half, plane):
        for piece in PIECES:
            own_copy(layer, flow, half, piece, plane).wait_send()

    def drain_slot(slot):
        for k in range(CHUNKS):
            ag_copy(slot, 0, k, t, t2).wait_send()
            ag_copy(slot, 1, k, t, t1).wait_send()
            ag_copy(slot, 2, k, t2, t1).wait_send()
            rs_copy(slot, k).wait_send()
        px_copy(slot, c).wait_send()

    def drain_blocks(layer):
        for k in range(3):
            for piece in PIECES:
                def act(k=k, piece=piece):
                    for unit in UNITS[piece]:
                        if k == 0:
                            near_copy(layer, blocks[0], unit).wait_send()
                        else:
                            across_copy(layer, k, blocks[k], unit).wait_send()

                            @pl.when(jnp.logical_and(is_mid, layer > 0))
                            def _(unit=unit):
                                outer_copy(layer, k, blocks[k], unit).wait_send()
                holds(blocks[k], piece, act)

    def drain(layer, _):
        @pl.when(jnp.logical_and(c != s_parity, jnp.logical_or(is_mid, layer > 0)))
        def _():
            bx_copy(layer).wait_send()

        @pl.when(is_end)
        def _():
            drain_own(layer, 0, g, mid_here)
            drain_own(layer, 1, other, mid_here)

        @pl.when(is_mid)
        def _():
            drain_own(layer, 0, g, mid_far)

            @pl.when(layer > 0)
            def _():
                drain_own(layer, 1, g, end_here)

        @pl.when(jnp.logical_or(is_mid, layer > 0))
        def _():
            drain_blocks(layer)
            drain_slot(layer)
        up_ok = jnp.logical_and(s < last, jnp.logical_or(layer > 0, s == 1))
        down_ok = jnp.logical_and(s > 0, jnp.logical_or(layer > 0, s == 2))
        halo_do(layer, 0, up_ok, lambda x: x.wait_send())
        halo_do(layer, 1, down_ok, lambda x: x.wait_send())
        return 0

    lax.fori_loop(0, LAYERS, drain, 0)

    @pl.when(is_mid)
    def _():
        drain_slot(GUEST)
        for k in range(CHUNKS):
            return_copy(k).wait_send()

    @pl.when(is_end)
    def _():
        for k in range(CHUNKS):
            guest_copy(k).wait_send()


def fused(tokens_in, norm_gain, w_pool_in, w_gate, w_back):
    sp_count, tp_count = lax.axis_size("sp"), lax.axis_size("tp")
    toks, feats = tokens_in.shape
    _, depth, local_pool = w_pool_in.shape
    b_rows, b_cols = w_back.shape[1:]
    cols_k = feats // CHUNKS
    bf, f32 = jnp.bfloat16, jnp.float32
    dma = pltpu.SemaphoreType.DMA
    slots = LAYERS + 1
    hbm = pl.BlockSpec(memory_space=pltpu.HBM)
    vmem = pl.BlockSpec(memory_space=pltpu.VMEM)
    return pl.pallas_call(
        functools.partial(fused_kernel, sp_count, tp_count),
        out_shape=jax.ShapeDtypeStruct((toks, feats), bf),
        in_specs=[hbm, vmem, hbm, hbm, hbm],
        out_specs=vmem,
        scratch_shapes=[
            pltpu.VMEM((LAYERS, sp_count * depth, local_pool), bf),
            pltpu.VMEM((LAYERS, sp_count * depth, w_gate.shape[2]), bf),
            pltpu.VMEM((LAYERS, 2, 2 * b_rows, b_cols), bf),
            pltpu.VMEM((LAYERS, b_rows, b_cols), bf),
            pltpu.VMEM((slots, tp_count, CHUNKS, toks, cols_k), bf),
            pltpu.VMEM((2, toks, tp_count * feats), bf),
            pltpu.VMEM((LAYERS, 3, toks, local_pool), bf),
            pltpu.VMEM((2, CHUNKS, toks, cols_k), f32),
            pltpu.VMEM((2, CHUNKS, toks, cols_k), f32),
            pltpu.VMEM((3, toks, toks), bf),
            pltpu.VMEM((2, toks, local_pool), f32),
            pltpu.VMEM((slots, 2, toks, local_pool), bf),
            pltpu.VMEM((slots, CHUNKS, toks, cols_k), bf),
            pltpu.VMEM((slots, CHUNKS, toks, cols_k), bf),
            pltpu.VMEM((CHUNKS, toks, cols_k), bf),
            dma((LAYERS + 1, 4)),
            dma((LAYERS, 7, 5)), dma((LAYERS, sp_count, 2, 5)),
            dma((LAYERS,)), dma((LAYERS,)),
            dma((CHUNKS,)), dma((CHUNKS,)), dma((CHUNKS,)), dma((CHUNKS,)),
            dma((slots, 3, CHUNKS)), dma((slots, 3, CHUNKS)),
            dma((LAYERS, 2)), dma((LAYERS, 2)),
            dma((slots,)), dma((slots,)),
            dma((slots, CHUNKS)), dma((slots, CHUNKS)),
        ],
        compiler_params=pltpu.CompilerParams(
            collective_id=0, has_side_effects=True, vmem_limit_bytes=56 * 1024 * 1024
        ),
    )(tokens_in, norm_gain, w_pool_in, w_gate, w_back)


def dispatch(tokens_in, norm_gain, w_pool_in, w_gate, w_back):
    fits = (
        lax.axis_size("grp") == 2
        and lax.axis_size("tp") == GROUPS == 4
        and lax.axis_size("sp") == lax.axis_size("tp")
        and w_pool_in.shape[2] * GROUPS == POOL_WIDTH
        and w_pool_in.shape[1] == tokens_in.shape[1]
        and tokens_in.shape[0] // GRID_W >= max(pool_windows) // 2
    )
    step = fused if fits else on_device
    return step(tokens_in, norm_gain, w_pool_in, w_gate, w_back)


def solution(mesh):
    return jax.shard_map(
        dispatch,
        mesh=mesh,
        in_specs=(
            P(("grp", "sp"), "tp"),
            P(),
            P(None, "sp", "tp"),
            P(None, "sp", "tp"),
            P(None, "tp", "sp"),
        ),
        out_specs=P(("grp", "sp"), "tp"),
        check_vma=False,
    )
```

time: 131 us -> 121 us (0.924)
  the two profiles are of different devices: /device:TPU:0 before, /device:TPU:3 now
where the time goes in v1:
time: 121 us; the launch traced here: 120 us
  Pallas kernels  119 us (98%)
  local copies, waits for them, and re-layouts  1.67 us (1%)
    pallas_call x1, Pallas kernels, fused(): pl.pallas_call(functools.partial(fused_kernel, sp_count, tp_count), out_s...  119 us

profile of v1, /device:TPU:3, one launch (start us, length us, event | category | flops | bytes accessed | tf_op | source)
XLA Modules:
  0.0 120.3 jit_solution(13010203540324014757)
XLA Ops:
  0.0 118.6 %shard_map.55 = bf16[256,512]{1,0:T(8,128)(2,1)} custom-call(bf16[256,512]{1,0:T(8,128)(2,1)} %tok_hbm.1, f32[3,2048]{1,0:T(4,128)} %gain_ref.1, bf16[3,512,256]{2,1,0:T(8,128)(2,1)} %wp_hbm.1, bf16[3,512,512]{2,1,0:T(8,128)(2,1)} %wg_hbm.1, bf16[3,256,512]{2,1,0:T(8,128)(2,1)} %wb_hbm.1), custom_call_target="tpu_custom_call" | custom-call | tf_op jit(solution)/shard_map/pallas_call | solution.py:747
  118.6 1.7 %copy.7 = bf16[256,512]{1,0:T(8,128)(2,1)} copy(bf16[256,512]{1,0:T(8,128)(2,1)} %shard_map.55) | data formatting | bytes 524288

commit v2 on v1

--- a/solution.py
+++ b/solution.py
@@ -120,12 +120,102 @@
 GUEST = LAYERS
 
 
+MID_FIRST = (
+    ("own", 0, 0, 0), ("own", 0, 0, 3), ("own", 1, 1, 0), ("gstart", 0), ("own", 1, 0, 2),
+    ("pump", 0, 0, 0), ("pump", 0, 1, 3), ("own", 2, 1, 3), ("own", 2, 1, 1), ("agf", 0, 0), ("guest", 0),
+    ("own", 2, 1, 0), ("pump", 1, 1, 2), ("own", 2, 1, 2), ("own", 1, 1, 2), ("agf", 0, 1),
+    ("pump", 0, 0, 3), ("pump", 0, 2, 3), ("own", 1, 1, 3), ("own", 1, 1, 1), ("pump", 0, 1, 0),
+    ("own", 0, 0, 2), ("guest", 1), ("pump", 0, 2, 0), ("own", 0, 0, 1), ("pool", 0), ("pump", 0, 0, 2),
+    ("pump", 0, 0, 1), ("pump", 0, 1, 2), ("own", 1, 0, 0), ("pump", 1, 0, 0), ("agf", 3, 0), ("agf", 3, 1),
+    ("pump", 0, 1, 1), ("pool", 3), ("pump", 0, 2, 2), ("pump", 0, 2, 1), ("box", 0), ("back", 3),
+    ("pump", 1, 1, 0), ("pump", 1, 2, 0), ("own", 1, 0, 1), ("pump", 1, 0, 1), ("back", 0), ("gate", 3),
+    ("upd", 3, 0), ("upd", 3, 1), ("own", 1, 0, 3), ("pump", 1, 0, 2), ("own", 2, 0, 3), ("pump", 1, 0, 3),
+    ("gate", 0), ("upd", 0, 0), ("pump", 1, 1, 1), ("own", 2, 0, 0), ("pump", 1, 2, 1), ("upd", 0, 1),
+)
+END_FIRST = (
+    ("own", 0, 0, 0), ("own", 0, 0, 3), ("tok", 0), ("tok", 1), ("pump", 1, 0, 0), ("own", 0, 0, 2),
+    ("own", 0, 1, 0), ("own", 0, 0, 1), ("pump", 1, 1, 2), ("own", 1, 0, 0), ("pump", 2, 0, 1),
+    ("own", 1, 0, 1), ("own", 0, 1, 3), ("own", 0, 1, 1), ("pump", 2, 0, 3), ("own", 0, 1, 2),
+    ("pump", 1, 0, 1), ("own", 1, 0, 3), ("own", 1, 0, 2), ("pump", 2, 0, 0), ("pump", 1, 0, 2),
+    ("pump", 1, 1, 0), ("own", 1, 1, 0), ("pump", 2, 0, 2), ("pump", 1, 0, 3), ("own", 2, 0, 0),
+    ("own", 2, 0, 1), ("own", 1, 1, 1), ("pump", 1, 2, 0), ("ret", 0), ("ret", 1),
+)
+MID_REST = (
+    (
+        ("pump", 1, 2, 3), ("pump", 1, 1, 3), ("pump", 2, 0, 0), ("pump", 1, 2, 2),
+    ),
+    (),
+    (
+        ("pump", 2, 1, 0), ("pump", 2, 2, 0),
+    ),
+    (
+        ("pump", 2, 0, 2), ("pump", 2, 0, 3), ("pump", 2, 1, 3), ("own", 2, 0, 1), ("pump", 2, 0, 1),
+    ),
+    (
+        ("pump", 2, 2, 2), ("pump", 2, 2, 3),
+    ),
+    (),
+    (),
+    (),
+    (
+        ("pump", 2, 1, 1), ("own", 2, 0, 2),
+    ),
+    (
+        ("pump", 2, 2, 1),
+    ),
+    (),
+    (
+        ("pump", 2, 1, 2),
+    ),
+    (),
+    (),
+    (),
+    (),
+)
+END_REST = (
+    (
+        ("pump", 1, 1, 1), ("pump", 1, 1, 3), ("own", 1, 1, 3),
+    ),
+    (
+        ("own", 2, 0, 2),
+    ),
+    (
+        ("pump", 1, 2, 3), ("pump", 1, 2, 2), ("own", 2, 0, 3), ("own", 1, 1, 2), ("own", 2, 1, 3),
+        ("pump", 1, 2, 1),
+    ),
+    (),
+    (),
+    (
+        ("own", 2, 1, 1), ("pump", 2, 1, 0), ("pump", 2, 1, 3), ("pump", 2, 2, 0),
+    ),
+    (),
+    (
+        ("own", 2, 1, 0), ("own", 2, 1, 2), ("pump", 2, 2, 2),
+    ),
+    (),
+    (
+        ("pump", 2, 2, 3),
+    ),
+    (
+        ("pump", 2, 1, 1), ("pump", 2, 2, 1),
+    ),
+    (),
+    (
+        ("pump", 2, 1, 2),
+    ),
+    (),
+    (),
+    (),
+)
+FIRST_BACK, FIRST_GATE = 3, 3
+
+
 def fused_kernel(
     sp_count, tp_count,
     tok_hbm, gain_ref, wp_hbm, wg_hbm, wb_hbm, out_ref,
     wp, wg, wb, wb_own, gathered, scaled, halo, gate_buf, own_part, box, counts,
     pair, parts, arrived, returned,
-    load_sem, w_send, w_recv, bx_send, bx_recv, tk_send, tk_recv, rt_send, rt_recv,
+    load_sem, w_send, z_recv, y_recv, bx_send, bx_recv, tk_send, tk_recv, rt_send, rt_recv,
     ag_send, ag_recv, h_send, h_recv, px_send, px_recv, rs_send, rs_recv,
 ):
     g = lax.axis_index("grp")
@@ -175,34 +265,35 @@
         row = unit - 3 if row is None else row
         return wb.at[layer, block // 2, pl.ds(pl.multiple_of(row * b_rows + half * n, n), n), :]
 
-    def w_copy(layer, flow, block, half, unit, target):
+    unit_rows = g_rows // 4
+
+    def units(sem, count):
+        ref = wg.at[pl.ds(0, -(-count // 16)), pl.ds(0, unit_rows * (count if count <= 16 else count // 2)), :]
+        return pltpu.make_async_remote_copy(
+            src_ref=ref, dst_ref=ref, send_sem=sem, recv_sem=sem,
+            device_id={"grp": other}, device_id_type=MESH,
+        )
+
+    def w_copy(layer, flow, block, half, unit, target, recv):
         ref = view(layer, block, half, unit)
         return pltpu.make_async_remote_copy(
-            src_ref=ref, dst_ref=ref,
-            send_sem=w_send.at[layer, flow, unit], recv_sem=w_recv.at[layer, block, half, unit],
+            src_ref=ref, dst_ref=ref, send_sem=w_send.at[flow], recv_sem=recv,
             device_id=target, device_id_type=MESH,
         )
 
-    def own_copy(layer, flow, half, piece, plane):
+    def kind(piece):
+        return {POOL: 0, GATE_A: 1, GATE_B: 1, BACK: 2}[piece]
+
+    def own_copy(layer, flow, half, piece, plane, recv):
         if piece != BACK:
-            return w_copy(layer, flow, s, half, UNITS[piece][0], {"sp": plane})
+            return w_copy(layer, flow, s, half, UNITS[piece][0], {"sp": plane}, recv)
         n = b_rows // 2
         return pltpu.make_async_remote_copy(
             src_ref=wb_own.at[layer, pl.ds(pl.multiple_of(half * n, n), n), :],
             dst_ref=view(layer, s, half, 3, row=c),
-            send_sem=w_send.at[layer, flow, 3], recv_sem=w_recv.at[layer, s, half, 3 + c],
+            send_sem=w_send.at[flow], recv_sem=recv,
             device_id={"sp": plane, "tp": base + s_parity}, device_id_type=MESH,
         )
-
-    def near_copy(layer, block, unit):
-        target = {"grp": jnp.where(is_mid, g, other), "sp": jnp.where(is_mid, mid_far, s)}
-        return w_copy(layer, 2, block, g, unit, target)
-
-    def across_copy(layer, k, block, unit):
-        return w_copy(layer, 2 + k, block, g, unit, {"grp": other})
-
-    def outer_copy(layer, k, block, unit):
-        return w_copy(layer, 4 + k, block, g, unit, {"sp": end_here})
 
     def holds(block, piece, fn):
         if piece == BACK:
@@ -210,27 +301,46 @@
         else:
             fn()
 
-    def pump(layer, k, *pieces):
+    def pump(mid, layer, k, piece):
         block = blocks[k]
-        for piece in pieces:
-            def act(piece=piece):
-                for unit in UNITS[piece]:
-                    w_copy(layer, 0, block, g, unit, {"grp": other}).wait_recv()
-                    if k == 0:
-                        near_copy(layer, block, unit).start()
-                    else:
-                        across_copy(layer, k, block, unit).start()
-
-                        @pl.when(jnp.logical_and(is_mid, layer > 0))
-                        def _(unit=unit):
-                            outer_copy(layer, k, block, unit).start()
-            holds(block, piece, act)
+
+        def act():
+            units(z_recv.at[layer, k, piece], len(UNITS[piece])).wait_recv()
+            for unit in UNITS[piece]:
+                if k == 0 and mid:
+                    w_copy(layer, 2, block, g, unit, {"sp": mid_far}, z_recv.at[layer, 2, piece]).start()
+                    continue
+                w_copy(
+                    layer, 2 + k, block, g, unit, {"grp": other}, y_recv.at[layer, kind(piece)]
+                ).start()
+                if mid and layer > 0:
+                    w_copy(
+                        layer, 4 + k, block, g, unit, {"sp": end_here}, z_recv.at[layer, k, piece]
+                    ).start()
+        holds(block, piece, act)
+
+    def own(mid, waited, layer, flow, piece):
+        if (layer, kind(piece)) not in waited:
+            waited.add((layer, kind(piece)))
+            load(layer, kind(piece)).wait()
+            if piece == BACK and (mid or layer > 0):
+                @pl.when(c != s_parity)
+                def _():
+                    bx_copy(layer).start()
+        if mid and flow == 0:
+            own_copy(layer, 0, g, piece, mid_far, z_recv.at[layer, 1, piece]).start()
+        elif mid:
+            own_copy(layer, 1, g, piece, end_here, z_recv.at[layer, 0, piece]).start()
+        elif flow == 0:
+            own_copy(layer, 0, g, piece, mid_here, z_recv.at[layer, 0, piece]).start()
+        else:
+            own_copy(layer, 1, other, piece, mid_here, y_recv.at[layer, kind(piece)]).start()
 
     def bx_copy(layer):
         return pltpu.make_async_remote_copy(
             src_ref=wb_own.at[layer],
             dst_ref=wb.at[layer, s // 2, pl.ds(pl.multiple_of(c * b_rows, b_rows), b_rows), :],
-            send_sem=bx_send.at[layer], recv_sem=bx_recv.at[layer],
+            send_sem=bx_send.at[0], recv_sem=bx_recv.at[layer],
             device_id={"tp": t1}, device_id_type=MESH,
         )
 
@@ -250,25 +360,20 @@
             src, dst = wb_hbm.at[layer], wb_own.at[layer]
         return pltpu.make_async_copy(src, dst, load_sem.at[layer, piece])
 
-    def ready(layer, *pieces):
-        for piece in pieces:
-            for k in range(3):
-                block = blocks[k]
-
-                def act(piece=piece, block=block):
-                    for unit in UNITS[piece]:
-                        w_copy(layer, 0, block, other, unit, {"grp": other}).wait_recv()
-                holds(block, piece, act)
-            if piece == BACK:
-                @pl.when(c == s_parity)
-                def _():
-                    wb_load(layer).wait()
-                    pltpu.make_async_remote_copy(
-                        src_ref=wb_own.at[layer],
-                        dst_ref=wb.at[layer, s // 2, pl.ds(pl.multiple_of((1 - c) * b_rows, b_rows), b_rows), :],
-                        send_sem=bx_send.at[layer], recv_sem=bx_recv.at[layer],
-                        device_id={"tp": t1}, device_id_type=MESH,
-                    ).wait_recv()
+    def ready(layer, which):
+        if which < 2:
+            units(y_recv.at[layer, which], 3 * (1 + which)).wait_recv()
+            return
+
+        @pl.when(c == s_parity)
+        def _():
+            units(y_recv.at[layer, 2], 2).wait_recv()
+            wb_load(layer).wait()
+            units(bx_recv.at[layer], 2).wait_recv()
+
+        @pl.when(c != s_parity)
+        def _():
+            units(y_recv.at[layer, 2], 4).wait_recv()
 
     def tok_load(k):
         return pltpu.make_async_copy(
@@ -278,27 +383,31 @@
     def guest_copy(k):
         return pltpu.make_async_remote_copy(
             src_ref=gathered.at[0, t, k], dst_ref=gathered.at[GUEST, t, k],
-            send_sem=tk_send.at[k], recv_sem=tk_recv.at[k],
+            send_sem=tk_send.at[0], recv_sem=tk_recv.at[k],
             device_id={"sp": mid_here}, device_id_type=MESH,
         )
 
     def return_copy(k):
         return pltpu.make_async_remote_copy(
             src_ref=returned.at[k], dst_ref=gathered.at[1, t, k],
-            send_sem=rt_send.at[k], recv_sem=rt_recv.at[k],
+            send_sem=rt_send.at[0], recv_sem=rt_recv.at[k],
             device_id={"sp": end_here}, device_id_type=MESH,
         )
 
-    def ag_copy(slot, which, k, block, target):
+    def ag_copy(slot, k, block, target, recv):
         return pltpu.make_async_remote_copy(
             src_ref=gathered.at[slot, block, k], dst_ref=gathered.at[slot, block, k],
-            send_sem=ag_send.at[slot, which, k], recv_sem=ag_recv.at[slot, which, k],
+            send_sem=ag_send.at[0], recv_sem=ag_recv.at[slot, recv],
             device_id={"tp": target}, device_id_type=MESH,
         )
 
     def start_gather(slot, k):
-        ag_copy(slot, 0, k, t, t2).start()
-        ag_copy(slot, 1, k, t, t1).start()
+        ag_copy(slot, k, t, t2, k).start()
+        ag_copy(slot, k, t, t1, 3).start()
+
+    def pass_on(slot, k):
+        units(ag_recv.at[slot, k], 1).wait_recv()
+        ag_copy(slot, k, t2, t1, 2).start()
 
     spans = [w // 2 for w in pool_windows]
 
@@ -333,14 +442,14 @@
     def px_copy(slot, row):
         return pltpu.make_async_remote_copy(
             src_ref=pair.at[slot, row], dst_ref=pair.at[slot, row],
-            send_sem=px_send.at[slot], recv_sem=px_recv.at[slot],
+            send_sem=px_send.at[0], recv_sem=px_recv.at[slot],
             device_id={"tp": t1}, device_id_type=MESH,
         )
 
     def rs_copy(slot, k):
         return pltpu.make_async_remote_copy(
             src_ref=parts.at[slot, k], dst_ref=arrived.at[slot, k],
-            send_sem=rs_send.at[slot, k], recv_sem=rs_recv.at[slot, k],
+            send_sem=rs_send.at[0], recv_sem=rs_recv.at[slot, k],
             device_id={"tp": t2}, device_id_type=MESH,
         )
 
@@ -378,7 +487,7 @@
         )
 
     def back(layer, slot, which):
-        px_copy(slot, 1 - c).wait_recv()
+        units(px_recv.at[slot], 1).wait_recv()
         for k in range(CHUNKS):
             parts[slot, k] = back_part(layer, slot, far_base // 2, k).astype(bf)
             rs_copy(slot, k).start()
@@ -386,7 +495,7 @@
             own_part[which, k] = back_part(layer, slot, base // 2, k)
 
     def update(slot, which, k):
-        rs_copy(slot, k).wait_recv()
+        units(rs_recv.at[slot, k], 1).wait_recv()
         branch = own_part[which, k] + arrived[slot, k].astype(f32)
         return (gathered[slot, t, k].astype(f32) + gate_buf[which, k] * branch).astype(bf)
 
@@ -418,26 +527,6 @@
             pl.semaphore_signal(barrier, inc=1, device_id={"sp": s + 1, "tp": peer}, device_id_type=MESH)
 
     pl.semaphore_wait(barrier, 3 + jnp.where(s > 0, 2, 0) + jnp.where(s < last, 2, 0))
-
-    def own_loads(layer):
-        for piece in (0, 2, 1):
-            load(layer, piece).wait()
-
-        @pl.when(c != s_parity)
-        def _():
-            bx_copy(layer).start()
-
-    PIECES = (POOL, BACK, GATE_A, GATE_B)
-
-    def end_own(layer, mine, *pieces):
-        for piece in pieces:
-            half = g if mine else other
-            own_copy(layer, 0 if mine else 1, half, piece, mid_here).start()
-
-    def mid_own(layer, flow, *pieces):
-        plane = mid_far if flow == 0 else end_here
-        for piece in pieces:
-            own_copy(layer, flow, g, piece, plane).start()
 
     def setup():
         half_span = jnp.int32(spans[0])
@@ -467,270 +556,185 @@
 
     for k in range(CHUNKS):
         tok_load(k).wait()
+    waited_mid, waited_end = set(), set()
+    zero = jnp.zeros((toks, 1), f32)
+
+    def relay(mid, item):
+        if item[0] == "own":
+            own(mid, waited_mid if mid else waited_end, *item[1:])
+        else:
+            pump(mid, *item[1:])
+
+    def gather_step(layer, slot, which, k, total):
+        if k == 0:
+            total = absorb(layer, slot, which, t, zero)
+            units(ag_recv.at[slot, 3], 2).wait_recv()
+            total = absorb(layer, slot, which, t1, total)
+        pass_on(slot, k)
+        if k == CHUNKS - 1:
+            total = absorb(layer, slot, which, t2, total)
+        return total
+
+    def pool_step(layer, slot, which, total):
+        ready(layer, 0)
+        acc = half_dot(layer, which, base, wp)
+        units(ag_recv.at[slot, 2], 2).wait_recv()
+        total = absorb(layer, slot, which, t3, total)
+        scale = scale_of(total)
+        acc = acc + half_dot(layer, which, far_base, wp)
+        return (acc * scale).astype(bf), scale
 
     @pl.when(is_end)
     def _():
-        load(0, 0).wait()
-        end_own(0, True, POOL)
-        for k in range(CHUNKS):
-            guest_copy(k).start()
-        end_own(0, False, POOL)
-        load(0, 2).wait()
-        end_own(0, True, BACK)
-        load(0, 1).wait()
-        end_own(0, True, GATE_A, GATE_B)
-        end_own(0, False, BACK, GATE_A, GATE_B)
-        own_loads(1)
-        own_loads(2)
-        setup()
-        pump(1, 0, POOL, BACK, GATE_A, GATE_B)
-        pump(2, 0, POOL)
-        end_own(1, True, POOL, BACK)
-        pump(2, 0, BACK, GATE_A, GATE_B)
-        end_own(1, True, GATE_A, GATE_B)
-        end_own(1, False, POOL, BACK)
-        for k in range(CHUNKS):
-            return_copy(k).wait_recv()
-            start_gather(1, k)
-        pump(1, 1, POOL)
+        for item in END_FIRST:
+            if item[0] == "tok":
+                guest_copy(item[1]).start()
+            elif item[0] == "ret":
+                if item[1] == 0:
+                    setup()
+                return_copy(item[1]).wait_recv()
+                start_gather(1, item[1])
+            else:
+                relay(False, item)
 
     @pl.when(is_mid)
     def _():
         guest_side = jnp.where(low, 0, 2)
+        total, scale = {}, {}
+        for item in MID_FIRST:
+            name = item[0]
+            slot = item[1]
+            which = 1 if slot == GUEST else 0
+            if name == "gstart":
+                for k in range(CHUNKS):
+                    start_gather(0, k)
+            elif name == "guest":
+                guest_copy(slot).wait_recv()
+                start_gather(GUEST, slot)
+            elif name == "agf":
+                if item == ("agf", 0, 0):
+                    setup()
+                total[slot] = gather_step(0, slot, which, item[2], total.get(slot))
+            elif name == "pool" and slot == 0:
+                halo[0, 1], scale[0] = pool_step(0, 0, 0, total[0])
+                halo_start(0)
+            elif name == "pool":
+                units(ag_recv.at[GUEST, 2], 2).wait_recv()
+                total[slot] = absorb(0, GUEST, 1, t3, total[slot])
+                scale[slot] = scale_of(total[slot])
+                acc = half_dot(0, 1, base, wp) + half_dot(0, 1, far_base, wp)
+                halo[0, guest_side] = (acc * scale[slot]).astype(bf)
+                cells = halo[0, guest_side]
+                sums = box_dot(1, cells) + box_dot(2 - guest_side, halo[0, 1])
+                share_pooled(GUEST, 1, sums, cells)
+            elif name == "box":
+                halo_wait(0)
+                cells = halo[0, 1]
+                sums = box_dot(0, halo[0, 0]) + box_dot(1, cells) + box_dot(2, halo[0, 2])
+                share_pooled(0, 0, sums, cells)
+            elif name == "back":
+                if slot == FIRST_BACK:
+                    ready(0, 2)
+                back(0, slot, which)
+            elif name == "gate":
+                if slot == FIRST_GATE:
+                    ready(0, 1)
+                gate_of(0, which, scale[slot])
+            elif name == "upd":
+                k = item[2]
+                value = update(slot, which, k)
+                if slot == GUEST:
+                    returned[k] = value
+                    return_copy(k).start()
+                else:
+                    gathered[1, t, k] = value
+                    start_gather(1, k)
+            else:
+                relay(True, item)
+
+    steps = iter(zip(MID_REST, END_REST))
+
+    def relays():
+        for mid, items in zip((True, False), next(steps)):
+            if items:
+                @pl.when(is_mid if mid else is_end)
+                def _(mid=mid, items=items):
+                    for item in items:
+                        relay(mid, item)
+
+    for layer in range(1, LAYERS):
+        total = None
         for k in range(CHUNKS):
-            start_gather(0, k)
-        load(0, 0).wait()
-        mid_own(0, 0, POOL)
-        load(0, 2).wait()
-        mid_own(0, 0, BACK)
-        load(0, 1).wait()
-        mid_own(0, 0, GATE_A, GATE_B)
-
-        @pl.when(c != s_parity)
-        def _():
-            bx_copy(0).start()
-        own_loads(1)
-        own_loads(2)
-        mid_own(1, 1, *PIECES)
-        mid_own(2, 1, *PIECES)
-        zero = jnp.zeros((toks, 1), f32)
-        total = absorb(0, 0, 0, t, zero)
-        pump(0, 1, POOL)
-        pump(0, 0, POOL)
-        setup()
-        for k in range(CHUNKS):
-            guest_copy(k).wait_recv()
-            start_gather(GUEST, k)
-        for k in range(CHUNKS):
-            ag_copy(0, 1, k, t1, t1).wait_recv()
-            ag_copy(0, 0, k, t2, t2).wait_recv()
-            ag_copy(0, 2, k, t2, t1).start()
-        total = absorb(0, 0, 0, t1, total)
-        pump(0, 1, BACK)
-        pump(0, 2, POOL)
-        total = absorb(0, 0, 0, t2, total)
-        for k in range(CHUNKS):
-            ag_copy(0, 2, k, t3, t1).wait_recv()
-        total = absorb(0, 0, 0, t3, total)
-        scale = scale_of(total)
-        guest_total = absorb(0, GUEST, 1, t, zero)
-        pump(0, 1, GATE_A)
-        for k in range(CHUNKS):
-            ag_copy(GUEST, 1, k, t1, t1).wait_recv()
-            ag_copy(GUEST, 0, k, t2, t2).wait_recv()
-            ag_copy(GUEST, 2, k, t2, t1).start()
-        pump(0, 0, BACK)
-        guest_total = absorb(0, GUEST, 1, t1, guest_total)
-        guest_total = absorb(0, GUEST, 1, t2, guest_total)
-        ready(0, POOL)
-        acc = half_dot(0, 0, base, wp) + half_dot(0, 0, far_base, wp)
-        halo[0, 1] = (acc * scale).astype(bf)
-        halo_start(0)
-        for k in range(CHUNKS):
-            ag_copy(GUEST, 2, k, t3, t1).wait_recv()
-        guest_total = absorb(0, GUEST, 1, t3, guest_total)
-        guest_scale = scale_of(guest_total)
-        acc = half_dot(0, 1, base, wp) + half_dot(0, 1, far_base, wp)
-        halo[0, guest_side] = (acc * guest_scale).astype(bf)
-        cells = halo[0, guest_side]
-        own_cells = halo[0, 1]
-        share_pooled(GUEST, 1, box_dot(1, cells) + box_dot(2 - guest_side, own_cells), cells)
-        pump(0, 1, GATE_B)
-        pump(0, 0, GATE_A)
-        pump(0, 2, BACK)
-        halo_wait(0)
-        sums = box_dot(0, halo[0, 0]) + box_dot(1, own_cells) + box_dot(2, halo[0, 2])
-        share_pooled(0, 0, sums, own_cells)
-        pump(0, 0, GATE_B)
-        mid_own(1, 0, *PIECES)
-        ready(0, BACK)
-        back(0, GUEST, 1)
-        back(0, 0, 0)
-        pump(0, 2, GATE_A, GATE_B)
-        ready(0, GATE_A, GATE_B)
-        gate_of(0, 1, guest_scale)
-        for k in range(CHUNKS):
-            returned[k] = update(GUEST, 1, k)
-            return_copy(k).start()
-        gate_of(0, 0, scale)
-        for k in range(CHUNKS):
-            gathered[1, t, k] = update(0, 0, k)
-            start_gather(1, k)
-        pump(1, 1, POOL)
-
-    def one_layer(layer, _):
-        more = layer + 1 < LAYERS
-        @pl.when(jnp.logical_and(is_mid, layer == 1))
-        def _():
-            pump(layer, 0, POOL)
-        pump(layer, 2, POOL)
-        total = absorb(layer, layer, 0, t, jnp.zeros((toks, 1), f32))
-        pump(layer, 1, BACK)
-        for k in range(CHUNKS):
-            ag_copy(layer, 1, k, t1, t1).wait_recv()
-        total = absorb(layer, layer, 0, t1, total)
-        for k in range(CHUNKS):
-            ag_copy(layer, 0, k, t2, t2).wait_recv()
-            ag_copy(layer, 2, k, t2, t1).start()
-        total = absorb(layer, layer, 0, t2, total)
-        ready(layer, POOL)
-        acc = half_dot(layer, 0, base, wp)
-        for k in range(CHUNKS):
-            ag_copy(layer, 2, k, t3, t1).wait_recv()
-        total = absorb(layer, layer, 0, t3, total)
-        scale = scale_of(total)
-        acc = acc + half_dot(layer, 0, far_base, wp)
-        halo[layer, 1] = (acc * scale).astype(bf)
+            total = gather_step(layer, layer, 0, k, total)
+            relays()
+        cells, scale = pool_step(layer, layer, 0, total)
+        halo[layer, 1] = cells
         halo_start(layer)
-
-        @pl.when(is_end)
-        def _():
-            end_own(layer, False, GATE_A, GATE_B)
-
-            @pl.when(more)
-            def _():
-                end_own(layer + 1, True, POOL, BACK)
-                end_own(layer + 1, False, POOL, BACK)
-                end_own(layer + 1, True, GATE_A, GATE_B)
-
-        @pl.when(is_mid)
-        def _():
-            pump(layer, 0, BACK)
-        pump(layer, 2, BACK)
-
-        @pl.when(is_mid)
-        def _():
-            pump(layer, 0, GATE_A)
-        pump(layer, 1, GATE_A)
+        relays()
         cells = halo[layer, 1]
         sums = box_dot(1, cells)
         halo_wait(layer)
         sums = sums + box_dot(0, halo[layer, 0]) + box_dot(2, halo[layer, 2])
         share_pooled(layer, 0, sums, cells)
-
-        @pl.when(is_mid)
-        def _():
-            pump(layer, 0, GATE_B)
-        pump(layer, 1, GATE_B)
-
-        @pl.when(jnp.logical_and(is_mid, more))
-        def _():
-            mid_own(layer + 1, 0, *PIECES)
-        ready(layer, BACK)
+        relays()
+        ready(layer, 2)
         back(layer, layer, 0)
-        pump(layer, 2, GATE_A, GATE_B)
-
-        @pl.when(more)
-        def _():
-            pump(layer + 1, 1, POOL)
-
-            @pl.when(is_mid)
-            def _():
-                pump(layer + 1, 0, POOL)
-        ready(layer, GATE_A, GATE_B)
+        relays()
+        ready(layer, 1)
         gate_of(layer, 0, scale)
+        relays()
         for k in range(CHUNKS):
             state = update(layer, 0, k)
-
-            @pl.when(more)
-            def _(k=k, state=state):
+            if layer + 1 < LAYERS:
                 gathered[layer + 1, t, k] = state
                 start_gather(layer + 1, k)
-
-            @pl.when(jnp.logical_not(more))
-            def _(k=k, state=state):
+            else:
                 out_ref[:, k * cols_k:(k + 1) * cols_k] = state
-        return 0
-
-    lax.fori_loop(1, LAYERS, one_layer, 0)
-
-    def drain_own(layer, flow, half, plane):
-        for piece in PIECES:
-            own_copy(layer, flow, half, piece, plane).wait_send()
-
-    def drain_slot(slot):
-        for k in range(CHUNKS):
-            ag_copy(slot, 0, k, t, t2).wait_send()
-            ag_copy(slot, 1, k, t, t1).wait_send()
-            ag_copy(slot, 2, k, t2, t1).wait_send()
-            rs_copy(slot, k).wait_send()
-        px_copy(slot, c).wait_send()
-
-    def drain_blocks(layer):
-        for k in range(3):
-            for piece in PIECES:
-                def act(k=k, piece=piece):
-                    for unit in UNITS[piece]:
-                        if k == 0:
-                            near_copy(layer, blocks[0], unit).wait_send()
-                        else:
-                            across_copy(layer, k, blocks[k], unit).wait_send()
-
-                            @pl.when(jnp.logical_and(is_mid, layer > 0))
-                            def _(unit=unit):
-                                outer_copy(layer, k, blocks[k], unit).wait_send()
-                holds(blocks[k], piece, act)
-
-    def drain(layer, _):
-        @pl.when(jnp.logical_and(c != s_parity, jnp.logical_or(is_mid, layer > 0)))
+            relays()
+
+    def sent(sem, count):
+        units(sem, count).wait_send()
+
+    def sent_blocks(flow, k, layers):
+        @pl.when(c == blocks[k] % 2)
         def _():
-            bx_copy(layer).wait_send()
-
-        @pl.when(is_end)
+            sent(w_send.at[flow], 5 * layers)
+
+        @pl.when(c != blocks[k] % 2)
         def _():
-            drain_own(layer, 0, g, mid_here)
-            drain_own(layer, 1, other, mid_here)
-
-        @pl.when(is_mid)
+            sent(w_send.at[flow], 3 * layers)
+
+    def sent_chain(layers, slots):
+        @pl.when(c != s_parity)
         def _():
-            drain_own(layer, 0, g, mid_far)
-
-            @pl.when(layer > 0)
-            def _():
-                drain_own(layer, 1, g, end_here)
-
-        @pl.when(jnp.logical_or(is_mid, layer > 0))
-        def _():
-            drain_blocks(layer)
-            drain_slot(layer)
-        up_ok = jnp.logical_and(s < last, jnp.logical_or(layer > 0, s == 1))
-        down_ok = jnp.logical_and(s > 0, jnp.logical_or(layer > 0, s == 2))
-        halo_do(layer, 0, up_ok, lambda x: x.wait_send())
-        halo_do(layer, 1, down_ok, lambda x: x.wait_send())
-        return 0
-
-    lax.fori_loop(0, LAYERS, drain, 0)
+            sent(bx_send.at[0], 2 * layers)
+        sent(ag_send.at[0], 6 * slots)
+        sent(rs_send.at[0], 2 * slots)
+        sent(px_send.at[0], slots)
 
     @pl.when(is_mid)
     def _():
-        drain_slot(GUEST)
-        for k in range(CHUNKS):
-            return_copy(k).wait_send()
+        sent(w_send.at[0], 4 * LAYERS)
+        sent(w_send.at[1], 4 * (LAYERS - 1))
+        for k in range(3):
+            sent_blocks(2 + k, k, LAYERS)
+        for k in (1, 2):
+            sent_blocks(4 + k, k, LAYERS - 1)
+        sent(rt_send.at[0], CHUNKS)
+        sent_chain(LAYERS, LAYERS + 1)
 
     @pl.when(is_end)
     def _():
-        for k in range(CHUNKS):
-            guest_copy(k).wait_send()
+        sent(w_send.at[0], 4 * LAYERS)
+        sent(w_send.at[1], 4 * LAYERS)
+        for k in range(3):
+            sent_blocks(2 + k, k, LAYERS - 1)
+        sent(tk_send.at[0], CHUNKS)
+        sent_chain(LAYERS - 1, LAYERS - 1)
+    for layer in range(LAYERS):
+        outward = layer > 0
+        halo_do(layer, 0, (s < last) if outward else (s == 1), lambda x: x.wait_send())
+        halo_do(layer, 1, (s > 0) if outward else (s == 2), lambda x: x.wait_send())
 
 
 def fused(tokens_in, norm_gain, w_pool_in, w_gate, w_back):
@@ -766,13 +770,13 @@
             pltpu.VMEM((slots, CHUNKS, toks, cols_k), bf),
             pltpu.VMEM((CHUNKS, toks, cols_k), bf),
             dma((LAYERS + 1, 4)),
-            dma((LAYERS, 7, 5)), dma((LAYERS, sp_count, 2, 5)),
-            dma((LAYERS,)), dma((LAYERS,)),
-            dma((CHUNKS,)), dma((CHUNKS,)), dma((CHUNKS,)), dma((CHUNKS,)),
-            dma((slots, 3, CHUNKS)), dma((slots, 3, CHUNKS)),
+            dma((7,)), dma((LAYERS, 3, 4)), dma((LAYERS, 3)),
+            dma((1,)), dma((LAYERS,)),
+            dma((1,)), dma((CHUNKS,)), dma((1,)), dma((CHUNKS,)),
+            dma((1,)), dma((slots, 4)),
             dma((LAYERS, 2)), dma((LAYERS, 2)),
-            dma((slots,)), dma((slots,)),
-            dma((slots, CHUNKS)), dma((slots, CHUNKS)),
+            dma((1,)), dma((slots,)),
+            dma((1,)), dma((slots, CHUNKS)),
         ],
         compiler_params=pltpu.CompilerParams(
             collective_id=0, has_side_effects=True, vmem_limit_bytes=56 * 1024 * 1024
@@ -786,7 +790,8 @@
         and lax.axis_size("tp") == GROUPS == 4
         and lax.axis_size("sp") == lax.axis_size("tp")
         and w_pool_in.shape[2] * GROUPS == POOL_WIDTH
-        and w_pool_in.shape[1] == tokens_in.shape[1]
+        and w_pool_in.shape[1] == tokens_in.shape[1] == w_gate.shape[2] == w_back.shape[2]
+        and tokens_in.shape[1] == 2 * tokens_in.shape[0] == 2 * w_pool_in.shape[2]
         and tokens_in.shape[0] // GRID_W >= max(pool_windows) // 2
     )
     step = fused if fits else on_device

time: 121 us -> 104 us (0.86)
  the two profiles are of different devices: /device:TPU:3 before, /device:TPU:0 now
where the time goes in v2:
time: 104 us
  Pallas kernels  102 us (98%)
  local copies, waits for them, and re-layouts  1.67 us (2%)
    pallas_call x1, Pallas kernels, fused(): pl.pallas_call(functools.partial(fused_kernel, sp_count, tp_count), out_s...  102 us

profile of v2, /device:TPU:0, one launch (start us, length us, event | category | flops | bytes accessed | tf_op | source)
XLA Modules:
  0.0 103.6 jit_solution(14138283077591412389)
XLA Ops:
  0.0 101.9 %shard_map.55 = bf16[256,512]{1,0:T(8,128)(2,1)} custom-call(bf16[256,512]{1,0:T(8,128)(2,1)} %tok_hbm.1, f32[3,2048]{1,0:T(4,128)} %gain_ref.1, bf16[3,512,256]{2,1,0:T(8,128)(2,1)} %wp_hbm.1, bf16[3,512,512]{2,1,0:T(8,128)(2,1)} %wg_hbm.1, bf16[3,256,512]{2,1,0:T(8,128)(2,1)} %wb_hbm.1), custom_call_target="tpu_custom_call" | custom-call | tf_op jit(solution)/shard_map/pallas_call | solution.py:751
  101.9 1.7 %copy.7 = bf16[256,512]{1,0:T(8,128)(2,1)} copy(bf16[256,512]{1,0:T(8,128)(2,1)} %shard_map.55) | data formatting | bytes 524288

commit v3 on v2

--- a/solution.py
+++ b/solution.py
@@ -121,87 +121,90 @@
 
 
 MID_FIRST = (
-    ("own", 0, 0, 0), ("own", 0, 0, 3), ("own", 1, 1, 0), ("gstart", 0), ("own", 1, 0, 2),
-    ("pump", 0, 0, 0), ("pump", 0, 1, 3), ("own", 2, 1, 3), ("own", 2, 1, 1), ("agf", 0, 0), ("guest", 0),
-    ("own", 2, 1, 0), ("pump", 1, 1, 2), ("own", 2, 1, 2), ("own", 1, 1, 2), ("agf", 0, 1),
-    ("pump", 0, 0, 3), ("pump", 0, 2, 3), ("own", 1, 1, 3), ("own", 1, 1, 1), ("pump", 0, 1, 0),
-    ("own", 0, 0, 2), ("guest", 1), ("pump", 0, 2, 0), ("own", 0, 0, 1), ("pool", 0), ("pump", 0, 0, 2),
-    ("pump", 0, 0, 1), ("pump", 0, 1, 2), ("own", 1, 0, 0), ("pump", 1, 0, 0), ("agf", 3, 0), ("agf", 3, 1),
-    ("pump", 0, 1, 1), ("pool", 3), ("pump", 0, 2, 2), ("pump", 0, 2, 1), ("box", 0), ("back", 3),
-    ("pump", 1, 1, 0), ("pump", 1, 2, 0), ("own", 1, 0, 1), ("pump", 1, 0, 1), ("back", 0), ("gate", 3),
-    ("upd", 3, 0), ("upd", 3, 1), ("own", 1, 0, 3), ("pump", 1, 0, 2), ("own", 2, 0, 3), ("pump", 1, 0, 3),
-    ("gate", 0), ("upd", 0, 0), ("pump", 1, 1, 1), ("own", 2, 0, 0), ("pump", 1, 2, 1), ("upd", 0, 1),
+    ("own", 1, 1, 1), ("own", 0, 0, 3), ("own", 0, 0, 0), ("own", 2, 0, 3), ("own", 1, 1, 2), ("gstart", 0),
+    ("own", 1, 0, 2), ("pump", 0, 1, 3), ("pump", 0, 0, 0), ("pump", 0, 1, 0), ("pump", 2, 1, 3),
+    ("guest", 0), ("own", 2, 1, 3), ("own", 1, 0, 3), ("own", 2, 1, 0), ("agf", 0, 0), ("agf", 0, 1),
+    ("own", 1, 0, 0), ("pump", 1, 1, 2), ("guest", 1), ("pump", 0, 2, 0), ("own", 0, 0, 1),
+    ("pump", 1, 1, 3), ("own", 2, 1, 1), ("pump", 1, 1, 0), ("agf", 3, 0), ("agf", 3, 1), ("pump", 0, 0, 3),
+    ("own", 1, 1, 3), ("own", 0, 0, 2), ("pool", 0), ("pump", 0, 0, 1), ("pump", 0, 1, 1),
+    ("pump", 0, 0, 2), ("pool", 3), ("own", 1, 0, 1), ("own", 2, 1, 2), ("pump", 0, 2, 3),
+    ("pump", 1, 0, 0), ("pump", 0, 1, 2), ("own", 1, 1, 0), ("box", 0), ("back", 3), ("pump", 0, 2, 1),
+    ("pump", 0, 2, 2), ("back", 0), ("pump", 2, 0, 0), ("pump", 1, 0, 3), ("pump", 1, 1, 1),
+    ("pump", 1, 2, 0), ("gate", 3), ("upd", 3, 0), ("upd", 3, 1), ("gate", 0), ("upd", 0, 0), ("upd", 0, 1),
+    ("pump", 1, 0, 2), ("pump", 1, 2, 3), ("pump", 1, 0, 1),
 )
 END_FIRST = (
-    ("own", 0, 0, 0), ("own", 0, 0, 3), ("tok", 0), ("tok", 1), ("pump", 1, 0, 0), ("own", 0, 0, 2),
-    ("own", 0, 1, 0), ("own", 0, 0, 1), ("pump", 1, 1, 2), ("own", 1, 0, 0), ("pump", 2, 0, 1),
-    ("own", 1, 0, 1), ("own", 0, 1, 3), ("own", 0, 1, 1), ("pump", 2, 0, 3), ("own", 0, 1, 2),
-    ("pump", 1, 0, 1), ("own", 1, 0, 3), ("own", 1, 0, 2), ("pump", 2, 0, 0), ("pump", 1, 0, 2),
-    ("pump", 1, 1, 0), ("own", 1, 1, 0), ("pump", 2, 0, 2), ("pump", 1, 0, 3), ("own", 2, 0, 0),
-    ("own", 2, 0, 1), ("own", 1, 1, 1), ("pump", 1, 2, 0), ("ret", 0), ("ret", 1),
+    ("tok", 0), ("own", 0, 0, 0), ("tok", 1), ("own", 0, 1, 2), ("own", 0, 0, 3), ("own", 0, 1, 0),
+    ("pump", 2, 1, 3), ("pump", 1, 0, 2), ("own", 0, 0, 2), ("pump", 1, 0, 1), ("own", 0, 0, 1),
+    ("pump", 1, 1, 2), ("pump", 2, 0, 3), ("own", 1, 0, 0), ("own", 0, 1, 3), ("own", 1, 0, 3),
+    ("own", 2, 0, 0), ("own", 0, 1, 1), ("pump", 1, 1, 3), ("own", 1, 0, 2), ("pump", 2, 0, 0),
+    ("own", 2, 0, 1), ("pump", 1, 1, 0), ("pump", 1, 0, 3), ("pump", 2, 0, 2), ("own", 1, 0, 1),
+    ("pump", 2, 0, 1), ("pump", 1, 2, 0), ("pump", 1, 0, 0), ("own", 1, 1, 0), ("own", 2, 0, 2),
+    ("own", 1, 1, 3), ("ret", 0), ("pump", 1, 1, 1), ("own", 2, 0, 3), ("ret", 1),
 )
 MID_REST = (
     (
-        ("pump", 1, 2, 3), ("pump", 1, 1, 3), ("pump", 2, 0, 0), ("pump", 1, 2, 2),
-    ),
-    (),
-    (
-        ("pump", 2, 1, 0), ("pump", 2, 2, 0),
-    ),
-    (
-        ("pump", 2, 0, 2), ("pump", 2, 0, 3), ("pump", 2, 1, 3), ("own", 2, 0, 1), ("pump", 2, 0, 1),
-    ),
-    (
-        ("pump", 2, 2, 2), ("pump", 2, 2, 3),
-    ),
-    (),
-    (),
-    (),
-    (
-        ("pump", 2, 1, 1), ("own", 2, 0, 2),
-    ),
-    (
-        ("pump", 2, 2, 1),
-    ),
-    (),
-    (
-        ("pump", 2, 1, 2),
-    ),
+        ("pump", 1, 2, 2),
+    ),
+    (
+        ("own", 2, 0, 0),
+    ),
+    (
+        ("pump", 2, 0, 1), ("pump", 1, 2, 1), ("pump", 2, 1, 0), ("pump", 2, 0, 3),
+    ),
+    (
+        ("pump", 2, 2, 0),
+    ),
+    (
+        ("pump", 2, 2, 1), ("pump", 2, 0, 2),
+    ),
+    (),
+    (
+        ("pump", 2, 2, 3),
+    ),
+    (
+        ("pump", 2, 2, 2), ("own", 2, 0, 2), ("pump", 2, 1, 2),
+    ),
+    (
+        ("own", 2, 0, 1),
+    ),
+    (),
+    (
+        ("pump", 2, 1, 1),
+    ),
+    (),
     (),
     (),
     (),
     (),
 )
 END_REST = (
-    (
-        ("pump", 1, 1, 1), ("pump", 1, 1, 3), ("own", 1, 1, 3),
-    ),
-    (
-        ("own", 2, 0, 2),
-    ),
-    (
-        ("pump", 1, 2, 3), ("pump", 1, 2, 2), ("own", 2, 0, 3), ("own", 1, 1, 2), ("own", 2, 1, 3),
-        ("pump", 1, 2, 1),
-    ),
-    (),
-    (),
-    (
-        ("own", 2, 1, 1), ("pump", 2, 1, 0), ("pump", 2, 1, 3), ("pump", 2, 2, 0),
-    ),
-    (),
-    (
-        ("own", 2, 1, 0), ("own", 2, 1, 2), ("pump", 2, 2, 2),
-    ),
-    (),
-    (
-        ("pump", 2, 2, 3),
-    ),
-    (
-        ("pump", 2, 1, 1), ("pump", 2, 2, 1),
-    ),
-    (),
-    (
-        ("pump", 2, 1, 2),
+    (),
+    (
+        ("pump", 1, 2, 3),
+    ),
+    (),
+    (
+        ("own", 1, 1, 1), ("pump", 1, 2, 2), ("pump", 1, 2, 1), ("own", 1, 1, 2),
+    ),
+    (
+        ("pump", 2, 1, 0),
+    ),
+    (
+        ("own", 2, 1, 0),
+    ),
+    (),
+    (
+        ("pump", 2, 2, 0), ("own", 2, 1, 1), ("pump", 2, 2, 3), ("pump", 2, 2, 1),
+    ),
+    (),
+    (),
+    (
+        ("pump", 2, 1, 2), ("own", 2, 1, 3), ("pump", 2, 2, 2), ("own", 2, 1, 2),
+    ),
+    (),
+    (
+        ("pump", 2, 1, 1),
     ),
     (),
     (),

time: 104 us -> 99.9 us (0.961)
  Pallas kernels: 102 us -> 98.1 us
    pallas_call x1, Pallas kernels: 102 us -> 98.1 us  [fused(): pl.pallas_call(functools.partial(fused_kernel, sp_count, tp_count), out_s...]
where the time goes in v3:
time: 99.9 us; the launch traced here: 99.7 us
  Pallas kernels  98.1 us (98%)
  local copies, waits for them, and re-layouts  1.67 us (2%)
    pallas_call x1, Pallas kernels, fused(): pl.pallas_call(functools.partial(fused_kernel, sp_count, tp_count), out_s...  98.1 us

profile of v3, /device:TPU:0, one launch (start us, length us, event | category | flops | bytes accessed | tf_op | source)
XLA Modules:
  0.0 99.7 jit_solution(8168615042360581520)
XLA Ops:
  0.0 98.1 %shard_map.55 = bf16[256,512]{1,0:T(8,128)(2,1)} custom-call(bf16[256,512]{1,0:T(8,128)(2,1)} %tok_hbm.1, f32[3,2048]{1,0:T(4,128)} %gain_ref.1, bf16[3,512,256]{2,1,0:T(8,128)(2,1)} %wp_hbm.1, bf16[3,512,512]{2,1,0:T(8,128)(2,1)} %wg_hbm.1, bf16[3,256,512]{2,1,0:T(8,128)(2,1)} %wb_hbm.1), custom_call_target="tpu_custom_call" | custom-call | tf_op jit(solution)/shard_map/pallas_call | solution.py:754
  98.1 1.7 %copy.7 = bf16[256,512]{1,0:T(8,128)(2,1)} copy(bf16[256,512]{1,0:T(8,128)(2,1)} %shard_map.55) | data formatting | bytes 524288

commit v4 on v3

--- a/solution.py
+++ b/solution.py
@@ -115,7 +115,8 @@
 
 MESH = pl.DeviceIdType.MESH
 POOL, GATE_A, GATE_B, BACK = range(4)
-UNITS = {POOL: (0,), GATE_A: (1,), GATE_B: (2,), BACK: (3, 4)}
+UNITS = {POOL: (0,), GATE_A: (1,), GATE_B: (2,), BACK: (3, 4), 4: (5,), 5: (6,)}
+GATE_PART = {1: 0, 2: 1, 5: 2, 6: 3}
 CHUNKS = 2
 GUEST = LAYERS
 
@@ -125,22 +126,23 @@
     ("own", 1, 0, 2), ("pump", 0, 1, 3), ("pump", 0, 0, 0), ("pump", 0, 1, 0), ("pump", 2, 1, 3),
     ("guest", 0), ("own", 2, 1, 3), ("own", 1, 0, 3), ("own", 2, 1, 0), ("agf", 0, 0), ("agf", 0, 1),
     ("own", 1, 0, 0), ("pump", 1, 1, 2), ("guest", 1), ("pump", 0, 2, 0), ("own", 0, 0, 1),
-    ("pump", 1, 1, 3), ("own", 2, 1, 1), ("pump", 1, 1, 0), ("agf", 3, 0), ("agf", 3, 1), ("pump", 0, 0, 3),
-    ("own", 1, 1, 3), ("own", 0, 0, 2), ("pool", 0), ("pump", 0, 0, 1), ("pump", 0, 1, 1),
-    ("pump", 0, 0, 2), ("pool", 3), ("own", 1, 0, 1), ("own", 2, 1, 2), ("pump", 0, 2, 3),
-    ("pump", 1, 0, 0), ("pump", 0, 1, 2), ("own", 1, 1, 0), ("box", 0), ("back", 3), ("pump", 0, 2, 1),
-    ("pump", 0, 2, 2), ("back", 0), ("pump", 2, 0, 0), ("pump", 1, 0, 3), ("pump", 1, 1, 1),
-    ("pump", 1, 2, 0), ("gate", 3), ("upd", 3, 0), ("upd", 3, 1), ("gate", 0), ("upd", 0, 0), ("upd", 0, 1),
-    ("pump", 1, 0, 2), ("pump", 1, 2, 3), ("pump", 1, 0, 1),
+    ("pump", 1, 1, 3), ("own", 2, 1, 1), ("own", 2, 1, 4), ("pump", 1, 1, 0), ("agf", 3, 0), ("agf", 3, 1),
+    ("pump", 0, 0, 3), ("own", 1, 1, 3), ("own", 0, 0, 2), ("pool", 0), ("pump", 0, 0, 1),
+    ("pump", 0, 1, 1), ("pump", 0, 0, 2), ("pool", 3), ("own", 1, 0, 1), ("own", 2, 1, 2), ("own", 2, 1, 5),
+    ("pump", 0, 2, 3), ("pump", 1, 0, 0), ("pump", 0, 1, 2), ("own", 1, 1, 0), ("box", 0), ("back", 3),
+    ("pump", 0, 2, 1), ("pump", 0, 2, 2), ("back", 0), ("pump", 2, 0, 0), ("pump", 1, 0, 3),
+    ("pump", 1, 1, 1), ("pump", 1, 2, 0), ("gate", 3), ("upd", 3, 0), ("upd", 3, 1), ("gate", 0),
+    ("upd", 0, 0), ("upd", 0, 1), ("pump", 1, 0, 2), ("pump", 1, 2, 3), ("pump", 1, 0, 1),
 )
 END_FIRST = (
     ("tok", 0), ("own", 0, 0, 0), ("tok", 1), ("own", 0, 1, 2), ("own", 0, 0, 3), ("own", 0, 1, 0),
     ("pump", 2, 1, 3), ("pump", 1, 0, 2), ("own", 0, 0, 2), ("pump", 1, 0, 1), ("own", 0, 0, 1),
     ("pump", 1, 1, 2), ("pump", 2, 0, 3), ("own", 1, 0, 0), ("own", 0, 1, 3), ("own", 1, 0, 3),
     ("own", 2, 0, 0), ("own", 0, 1, 1), ("pump", 1, 1, 3), ("own", 1, 0, 2), ("pump", 2, 0, 0),
-    ("own", 2, 0, 1), ("pump", 1, 1, 0), ("pump", 1, 0, 3), ("pump", 2, 0, 2), ("own", 1, 0, 1),
-    ("pump", 2, 0, 1), ("pump", 1, 2, 0), ("pump", 1, 0, 0), ("own", 1, 1, 0), ("own", 2, 0, 2),
-    ("own", 1, 1, 3), ("ret", 0), ("pump", 1, 1, 1), ("own", 2, 0, 3), ("ret", 1),
+    ("own", 2, 0, 1), ("own", 2, 0, 4), ("pump", 1, 1, 0), ("pump", 1, 0, 3), ("pump", 2, 0, 2),
+    ("pump", 2, 0, 5), ("own", 1, 0, 1), ("pump", 2, 0, 1), ("pump", 2, 0, 4), ("pump", 1, 2, 0),
+    ("pump", 1, 0, 0), ("own", 1, 1, 0), ("own", 2, 0, 2), ("own", 2, 0, 5), ("own", 1, 1, 3), ("ret", 0),
+    ("pump", 1, 1, 1), ("own", 2, 0, 3), ("ret", 1),
 )
 MID_REST = (
     (
@@ -150,27 +152,28 @@
         ("own", 2, 0, 0),
     ),
     (
-        ("pump", 2, 0, 1), ("pump", 1, 2, 1), ("pump", 2, 1, 0), ("pump", 2, 0, 3),
+        ("pump", 2, 0, 1), ("pump", 2, 0, 4), ("pump", 1, 2, 1), ("pump", 2, 1, 0), ("pump", 2, 0, 3),
     ),
     (
         ("pump", 2, 2, 0),
     ),
     (
-        ("pump", 2, 2, 1), ("pump", 2, 0, 2),
+        ("pump", 2, 2, 1), ("pump", 2, 2, 4), ("pump", 2, 0, 2), ("pump", 2, 0, 5),
     ),
     (),
     (
         ("pump", 2, 2, 3),
     ),
     (
-        ("pump", 2, 2, 2), ("own", 2, 0, 2), ("pump", 2, 1, 2),
-    ),
-    (
-        ("own", 2, 0, 1),
-    ),
-    (),
-    (
-        ("pump", 2, 1, 1),
+        ("pump", 2, 2, 2), ("pump", 2, 2, 5), ("own", 2, 0, 2), ("own", 2, 0, 5), ("pump", 2, 1, 2),
+        ("pump", 2, 1, 5),
+    ),
+    (
+        ("own", 2, 0, 1), ("own", 2, 0, 4),
+    ),
+    (),
+    (
+        ("pump", 2, 1, 1), ("pump", 2, 1, 4),
     ),
     (),
     (),
@@ -195,16 +198,18 @@
     ),
     (),
     (
-        ("pump", 2, 2, 0), ("own", 2, 1, 1), ("pump", 2, 2, 3), ("pump", 2, 2, 1),
-    ),
-    (),
-    (),
-    (
-        ("pump", 2, 1, 2), ("own", 2, 1, 3), ("pump", 2, 2, 2), ("own", 2, 1, 2),
-    ),
-    (),
-    (
-        ("pump", 2, 1, 1),
+        ("pump", 2, 2, 0), ("own", 2, 1, 1), ("own", 2, 1, 4), ("pump", 2, 2, 3), ("pump", 2, 2, 1),
+        ("pump", 2, 2, 4),
+    ),
+    (),
+    (),
+    (
+        ("pump", 2, 1, 2), ("pump", 2, 1, 5), ("own", 2, 1, 3), ("pump", 2, 2, 2), ("pump", 2, 2, 5),
+        ("own", 2, 1, 2), ("own", 2, 1, 5),
+    ),
+    (),
+    (
+        ("pump", 2, 1, 1), ("pump", 2, 1, 4),
     ),
     (),
     (),
@@ -215,10 +220,10 @@
 
 def fused_kernel(
     sp_count, tp_count,
-    tok_hbm, gain_ref, wp_hbm, wg_hbm, wb_hbm, out_ref,
+    tok_hbm, gain_hbm, wp_hbm, wg_hbm, wb_hbm, out_hbm,
     wp, wg, wb, wb_own, gathered, scaled, halo, gate_buf, own_part, box, counts,
-    pair, parts, arrived, returned,
-    load_sem, w_send, z_recv, y_recv, bx_send, bx_recv, tk_send, tk_recv, rt_send, rt_recv,
+    pair, parts, arrived, returned, gain_ref, final,
+    load_sem, w_send, z_recv, z_fine, y_recv, bx_send, bx_recv, tk_send, tk_recv, rt_send, rt_recv,
     ag_send, ag_recv, h_send, h_recv, px_send, px_recv, rs_send, rs_recv,
 ):
     g = lax.axis_index("grp")
@@ -256,13 +261,16 @@
     p_rows, g_rows = wp_hbm.shape[1], wg_hbm.shape[1]
     b_rows = wb_hbm.shape[1]
 
+    def gate_cuts(layer):
+        return 8 if layer == LAYERS - 1 else 4
+
     def view(layer, block, half, unit, row=None):
         if unit == 0:
             n = p_rows // 2
             return wp.at[layer, pl.ds(pl.multiple_of(block * p_rows + half * n, n), n), :]
-        if unit in (1, 2):
-            n = g_rows // 4
-            at = block * g_rows + half * (2 * n) + (unit - 1) * n
+        if unit in GATE_PART:
+            n = g_rows // gate_cuts(layer)
+            at = block * g_rows + half * (g_rows // 2) + GATE_PART[unit] * n
             return wg.at[layer, pl.ds(pl.multiple_of(at, n), n), :]
         n = b_rows // 2
         row = unit - 3 if row is None else row
@@ -271,7 +279,7 @@
     unit_rows = g_rows // 4
 
     def units(sem, count):
-        ref = wg.at[pl.ds(0, -(-count // 16)), pl.ds(0, unit_rows * (count if count <= 16 else count // 2)), :]
+        ref = wg.at[pl.ds(0, 2 if count > 16 else 1), pl.ds(0, int(unit_rows * (count if count <= 16 else count // 2))), :]
         return pltpu.make_async_remote_copy(
             src_ref=ref, dst_ref=ref, send_sem=sem, recv_sem=sem,
             device_id={"grp": other}, device_id_type=MESH,
@@ -285,7 +293,15 @@
         )
 
     def kind(piece):
-        return {POOL: 0, GATE_A: 1, GATE_B: 1, BACK: 2}[piece]
+        return {POOL: 0, BACK: 2}.get(piece, 1)
+
+    def z_sem(layer, k, piece):
+        return z_recv.at[layer, k, piece] if piece < 4 else z_fine.at[k, piece - 4]
+
+    def amount(layer, piece):
+        if piece == BACK:
+            return 2
+        return 1 if piece == POOL else 4 / gate_cuts(layer)
 
     def own_copy(layer, flow, half, piece, plane, recv):
         if piece != BACK:
@@ -308,17 +324,17 @@
         block = blocks[k]
 
         def act():
-            units(z_recv.at[layer, k, piece], len(UNITS[piece])).wait_recv()
+            units(z_sem(layer, k, piece), amount(layer, piece)).wait_recv()
             for unit in UNITS[piece]:
                 if k == 0 and mid:
-                    w_copy(layer, 2, block, g, unit, {"sp": mid_far}, z_recv.at[layer, 2, piece]).start()
+                    w_copy(layer, 2, block, g, unit, {"sp": mid_far}, z_sem(layer, 2, piece)).start()
                     continue
                 w_copy(
                     layer, 2 + k, block, g, unit, {"grp": other}, y_recv.at[layer, kind(piece)]
                 ).start()
                 if mid and layer > 0:
                     w_copy(
-                        layer, 4 + k, block, g, unit, {"sp": end_here}, z_recv.at[layer, k, piece]
+                        layer, 4 + k, block, g, unit, {"sp": end_here}, z_sem(layer, k, piece)
                     ).start()
         holds(block, piece, act)
 
@@ -331,11 +347,11 @@
                 def _():
                     bx_copy(layer).start()
         if mid and flow == 0:
-            own_copy(layer, 0, g, piece, mid_far, z_recv.at[layer, 1, piece]).start()
+            own_copy(layer, 0, g, piece, mid_far, z_sem(layer, 1, piece)).start()
         elif mid:
-            own_copy(layer, 1, g, piece, end_here, z_recv.at[layer, 0, piece]).start()
+            own_copy(layer, 1, g, piece, end_here, z_sem(layer, 0, piece)).start()
         elif flow == 0:
-            own_copy(layer, 0, g, piece, mid_here, z_recv.at[layer, 0, piece]).start()
+            own_copy(layer, 0, g, piece, mid_here, z_sem(layer, 0, piece)).start()
         else:
             own_copy(layer, 1, other, piece, mid_here, y_recv.at[layer, kind(piece)]).start()
 
@@ -383,6 +399,13 @@
             tok_hbm.at[:, pl.ds(k * cols_k, cols_k)], gathered.at[0, t, k], load_sem.at[LAYERS, k]
         )
 
+    gain_load = pltpu.make_async_copy(gain_hbm, gain_ref, load_sem.at[LAYERS, CHUNKS])
+
+    def out_copy(k):
+        return pltpu.make_async_copy(
+            final.at[k], out_hbm.at[:, pl.ds(k * cols_k, cols_k)], load_sem.at[0, k]
+        )
+
     def guest_copy(k):
         return pltpu.make_async_remote_copy(
             src_ref=gathered.at[0, t, k], dst_ref=gathered.at[GUEST, t, k],
@@ -504,6 +527,7 @@
 
     for k in range(CHUNKS):
         tok_load(k).start()
+    gain_load.start()
     for layer in range(LAYERS):
         for piece in (0, 2, 1):
             load(layer, piece).start()
@@ -559,6 +583,7 @@
 
     for k in range(CHUNKS):
         tok_load(k).wait()
+    gain_load.wait()
     waited_mid, waited_end = set(), set()
     zero = jnp.zeros((toks, 1), f32)
 
@@ -692,7 +717,8 @@
                 gathered[layer + 1, t, k] = state
                 start_gather(layer + 1, k)
             else:
-                out_ref[:, k * cols_k:(k + 1) * cols_k] = state
+                final[k] = state
+                out_copy(k).start()
             relays()
 
     def sent(sem, count):
@@ -738,6 +764,8 @@
         outward = layer > 0
         halo_do(layer, 0, (s < last) if outward else (s == 1), lambda x: x.wait_send())
         halo_do(layer, 1, (s > 0) if outward else (s == 2), lambda x: x.wait_send())
+    for k in range(CHUNKS):
+        out_copy(k).wait()
 
 
 def fused(tokens_in, norm_gain, w_pool_in, w_gate, w_back):
@@ -750,12 +778,11 @@
     dma = pltpu.SemaphoreType.DMA
     slots = LAYERS + 1
     hbm = pl.BlockSpec(memory_space=pltpu.HBM)
-    vmem = pl.BlockSpec(memory_space=pltpu.VMEM)
     return pl.pallas_call(
         functools.partial(fused_kernel, sp_count, tp_count),
         out_shape=jax.ShapeDtypeStruct((toks, feats), bf),
-        in_specs=[hbm, vmem, hbm, hbm, hbm],
-        out_specs=vmem,
+        in_specs=[hbm] * 5,
+        out_specs=hbm,
         scratch_shapes=[
             pltpu.VMEM((LAYERS, sp_count * depth, local_pool), bf),
             pltpu.VMEM((LAYERS, sp_count * depth, w_gate.shape[2]), bf),
@@ -772,8 +799,10 @@
             pltpu.VMEM((slots, CHUNKS, toks, cols_k), bf),
             pltpu.VMEM((slots, CHUNKS, toks, cols_k), bf),
             pltpu.VMEM((CHUNKS, toks, cols_k), bf),
+            pltpu.VMEM(norm_gain.shape, f32),
+            pltpu.VMEM((CHUNKS, toks, cols_k), bf),
             dma((LAYERS + 1, 4)),
-            dma((7,)), dma((LAYERS, 3, 4)), dma((LAYERS, 3)),
+            dma((7,)), dma((LAYERS, 3, 4)), dma((3, 2)), dma((LAYERS, 3)),
             dma((1,)), dma((LAYERS,)),
             dma((1,)), dma((CHUNKS,)), dma((1,)), dma((CHUNKS,)),
             dma((1,)), dma((slots, 4)),
@@ -785,7 +814,6 @@
             collective_id=0, has_side_effects=True, vmem_limit_bytes=56 * 1024 * 1024
         ),
     )(tokens_in, norm_gain, w_pool_in, w_gate, w_back)
-
 
 def dispatch(tokens_in, norm_gain, w_pool_in, w_gate, w_back):
     fits = (

time: 99.9 us -> 98.6 us (0.987)
  Pallas kernels: 98.1 us -> 96.5 us
    pallas_call x1, Pallas kernels: 98.1 us -> 96.5 us  [fused(): pl.pallas_call(functools.partial(fused_kernel, sp_count, tp_count), out_s...]
where the time goes in v4:
time: 98.6 us; the launch traced here: 98.2 us
  Pallas kernels  96.5 us (98%)
  local copies, waits for them, and re-layouts  1.67 us (2%)
    pallas_call x1, Pallas kernels, fused(): pl.pallas_call(functools.partial(fused_kernel, sp_count, tp_count), out_s...  96.5 us

profile of v4, /device:TPU:0, one launch (start us, length us, event | category | flops | bytes accessed | tf_op | source)
XLA Modules:
  0.0 98.2 jit_solution(18200194302749793356)
XLA Ops:
  0.0 96.5 %shard_map.55 = bf16[256,512]{1,0:T(8,128)(2,1)} custom-call(bf16[256,512]{1,0:T(8,128)(2,1)} %tok_hbm.1, f32[3,2048]{1,0:T(4,128)} %gain_hbm.1, bf16[3,512,256]{2,1,0:T(8,128)(2,1)} %wp_hbm.1, bf16[3,512,512]{2,1,0:T(8,128)(2,1)} %wg_hbm.1, bf16[3,256,512]{2,1,0:T(8,128)(2,1)} %wb_hbm.1), custom_call_target="tpu_custom_call" | custom-call | tf_op jit(solution)/shard_map/pallas_call | solution.py:781
  96.5 1.7 %copy.7 = bf16[256,512]{1,0:T(8,128)(2,1)} copy(bf16[256,512]{1,0:T(8,128)(2,1)} %shard_map.55) | data formatting | bytes 524288

commit v5 on v4

--- a/solution.py
+++ b/solution.py
@@ -122,58 +122,53 @@
 
 
 MID_FIRST = (
-    ("own", 1, 1, 1), ("own", 0, 0, 3), ("own", 0, 0, 0), ("own", 2, 0, 3), ("own", 1, 1, 2), ("gstart", 0),
-    ("own", 1, 0, 2), ("pump", 0, 1, 3), ("pump", 0, 0, 0), ("pump", 0, 1, 0), ("pump", 2, 1, 3),
-    ("guest", 0), ("own", 2, 1, 3), ("own", 1, 0, 3), ("own", 2, 1, 0), ("agf", 0, 0), ("agf", 0, 1),
-    ("own", 1, 0, 0), ("pump", 1, 1, 2), ("guest", 1), ("pump", 0, 2, 0), ("own", 0, 0, 1),
-    ("pump", 1, 1, 3), ("own", 2, 1, 1), ("own", 2, 1, 4), ("pump", 1, 1, 0), ("agf", 3, 0), ("agf", 3, 1),
-    ("pump", 0, 0, 3), ("own", 1, 1, 3), ("own", 0, 0, 2), ("pool", 0), ("pump", 0, 0, 1),
-    ("pump", 0, 1, 1), ("pump", 0, 0, 2), ("pool", 3), ("own", 1, 0, 1), ("own", 2, 1, 2), ("own", 2, 1, 5),
-    ("pump", 0, 2, 3), ("pump", 1, 0, 0), ("pump", 0, 1, 2), ("own", 1, 1, 0), ("box", 0), ("back", 3),
-    ("pump", 0, 2, 1), ("pump", 0, 2, 2), ("back", 0), ("pump", 2, 0, 0), ("pump", 1, 0, 3),
-    ("pump", 1, 1, 1), ("pump", 1, 2, 0), ("gate", 3), ("upd", 3, 0), ("upd", 3, 1), ("gate", 0),
-    ("upd", 0, 0), ("upd", 0, 1), ("pump", 1, 0, 2), ("pump", 1, 2, 3), ("pump", 1, 0, 1),
+    ("own", 1, 1, 0), ("own", 1, 0, 1), ("own", 0, 0, 2), ("own", 2, 1, 4), ("gstart", 0), ("own", 1, 1, 1),
+    ("own", 2, 1, 0), ("own", 0, 0, 0), ("own", 0, 0, 3), ("own", 2, 1, 5), ("pump", 0, 0, 3),
+    ("own", 1, 1, 3), ("own", 2, 1, 2), ("pump", 0, 0, 0), ("own", 1, 1, 2), ("pump", 1, 1, 1),
+    ("own", 0, 0, 1), ("pump", 0, 1, 0), ("guest", 0), ("pump", 0, 1, 3), ("own", 2, 1, 3),
+    ("pump", 0, 1, 2), ("guest", 1), ("agf", 0, 0), ("pump", 0, 2, 0), ("agf", 0, 1), ("pump", 0, 0, 1),
+    ("pump", 0, 0, 2), ("pump", 0, 2, 3), ("own", 2, 1, 1), ("agf", 3, 0), ("own", 1, 0, 0), ("agf", 3, 1),
+    ("pump", 0, 1, 1), ("pool", 0), ("pool", 3), ("pump", 1, 0, 3), ("pump", 0, 2, 1), ("pump", 0, 2, 2),
+    ("back", 3), ("pump", 1, 1, 0), ("box", 0), ("pump", 1, 2, 3), ("pump", 1, 0, 0), ("own", 1, 0, 3),
+    ("back", 0), ("gate", 3), ("upd", 3, 0), ("upd", 3, 1), ("own", 1, 0, 2), ("gate", 0),
+    ("pump", 1, 2, 0), ("upd", 0, 0), ("pump", 1, 0, 1), ("upd", 0, 1), ("pump", 1, 1, 3), ("own", 2, 0, 0),
+    ("pump", 1, 2, 1), ("pump", 1, 0, 2),
 )
 END_FIRST = (
-    ("tok", 0), ("own", 0, 0, 0), ("tok", 1), ("own", 0, 1, 2), ("own", 0, 0, 3), ("own", 0, 1, 0),
-    ("pump", 2, 1, 3), ("pump", 1, 0, 2), ("own", 0, 0, 2), ("pump", 1, 0, 1), ("own", 0, 0, 1),
-    ("pump", 1, 1, 2), ("pump", 2, 0, 3), ("own", 1, 0, 0), ("own", 0, 1, 3), ("own", 1, 0, 3),
-    ("own", 2, 0, 0), ("own", 0, 1, 1), ("pump", 1, 1, 3), ("own", 1, 0, 2), ("pump", 2, 0, 0),
-    ("own", 2, 0, 1), ("own", 2, 0, 4), ("pump", 1, 1, 0), ("pump", 1, 0, 3), ("pump", 2, 0, 2),
-    ("pump", 2, 0, 5), ("own", 1, 0, 1), ("pump", 2, 0, 1), ("pump", 2, 0, 4), ("pump", 1, 2, 0),
-    ("pump", 1, 0, 0), ("own", 1, 1, 0), ("own", 2, 0, 2), ("own", 2, 0, 5), ("own", 1, 1, 3), ("ret", 0),
-    ("pump", 1, 1, 1), ("own", 2, 0, 3), ("ret", 1),
+    ("own", 0, 0, 0), ("own", 0, 0, 3), ("tok", 0), ("tok", 1), ("own", 0, 1, 0), ("own", 0, 0, 1),
+    ("own", 0, 0, 2), ("own", 0, 1, 3), ("own", 1, 0, 3), ("own", 1, 0, 0), ("own", 0, 1, 2),
+    ("own", 0, 1, 1), ("own", 1, 0, 1), ("own", 1, 0, 2), ("pump", 1, 0, 0), ("own", 1, 1, 0),
+    ("own", 2, 0, 3), ("pump", 2, 0, 5), ("own", 2, 0, 0), ("pump", 1, 0, 2), ("pump", 1, 1, 1),
+    ("own", 1, 1, 3), ("pump", 2, 0, 2), ("pump", 1, 0, 3), ("pump", 1, 0, 1), ("pump", 2, 0, 3),
+    ("pump", 2, 0, 4), ("own", 2, 0, 4), ("own", 2, 0, 2), ("pump", 1, 2, 3), ("ret", 0), ("pump", 2, 0, 0),
+    ("pump", 1, 1, 0), ("ret", 1), ("pump", 1, 2, 0),
 )
 MID_REST = (
-    (
-        ("pump", 1, 2, 2),
-    ),
-    (
-        ("own", 2, 0, 0),
-    ),
-    (
-        ("pump", 2, 0, 1), ("pump", 2, 0, 4), ("pump", 1, 2, 1), ("pump", 2, 1, 0), ("pump", 2, 0, 3),
-    ),
-    (
-        ("pump", 2, 2, 0),
-    ),
-    (
-        ("pump", 2, 2, 1), ("pump", 2, 2, 4), ("pump", 2, 0, 2), ("pump", 2, 0, 5),
-    ),
-    (),
-    (
-        ("pump", 2, 2, 3),
-    ),
-    (
-        ("pump", 2, 2, 2), ("pump", 2, 2, 5), ("own", 2, 0, 2), ("own", 2, 0, 5), ("pump", 2, 1, 2),
-        ("pump", 2, 1, 5),
-    ),
-    (
-        ("own", 2, 0, 1), ("own", 2, 0, 4),
-    ),
-    (),
-    (
-        ("pump", 2, 1, 1), ("pump", 2, 1, 4),
+    (),
+    (),
+    (
+        ("pump", 2, 0, 0), ("pump", 2, 0, 3), ("pump", 1, 2, 2), ("pump", 1, 1, 2), ("own", 2, 0, 5),
+        ("own", 2, 0, 3),
+    ),
+    (
+        ("pump", 2, 1, 0),
+    ),
+    (
+        ("pump", 2, 2, 0), ("pump", 2, 2, 3), ("pump", 2, 0, 2), ("own", 2, 0, 2), ("pump", 2, 0, 4),
+        ("own", 2, 0, 4), ("pump", 2, 1, 3),
+    ),
+    (),
+    (),
+    (
+        ("pump", 2, 2, 4), ("pump", 2, 0, 5), ("own", 2, 0, 1), ("pump", 2, 0, 1), ("pump", 2, 2, 2),
+        ("pump", 2, 1, 2),
+    ),
+    (
+        ("pump", 2, 1, 4),
+    ),
+    (),
+    (
+        ("pump", 2, 2, 5), ("pump", 2, 2, 1), ("pump", 2, 1, 5), ("pump", 2, 1, 1),
     ),
     (),
     (),
@@ -182,34 +177,39 @@
     (),
 )
 END_REST = (
-    (),
-    (
-        ("pump", 1, 2, 3),
-    ),
-    (),
-    (
-        ("own", 1, 1, 1), ("pump", 1, 2, 2), ("pump", 1, 2, 1), ("own", 1, 1, 2),
-    ),
-    (
-        ("pump", 2, 1, 0),
-    ),
-    (
-        ("own", 2, 1, 0),
-    ),
-    (),
-    (
-        ("pump", 2, 2, 0), ("own", 2, 1, 1), ("own", 2, 1, 4), ("pump", 2, 2, 3), ("pump", 2, 2, 1),
-        ("pump", 2, 2, 4),
-    ),
-    (),
-    (),
-    (
-        ("pump", 2, 1, 2), ("pump", 2, 1, 5), ("own", 2, 1, 3), ("pump", 2, 2, 2), ("pump", 2, 2, 5),
-        ("own", 2, 1, 2), ("own", 2, 1, 5),
-    ),
-    (),
-    (
-        ("pump", 2, 1, 1), ("pump", 2, 1, 4),
+    (
+        ("pump", 1, 1, 3), ("pump", 2, 0, 1),
+    ),
+    (),
+    (
+        ("pump", 1, 2, 1), ("own", 1, 1, 2),
+    ),
+    (
+        ("pump", 1, 2, 2), ("own", 1, 1, 1),
+    ),
+    (
+        ("own", 2, 1, 1), ("pump", 1, 1, 2), ("own", 2, 0, 5), ("own", 2, 0, 1), ("pump", 2, 1, 0),
+        ("own", 2, 1, 5),
+    ),
+    (),
+    (
+        ("pump", 2, 2, 0), ("own", 2, 1, 0), ("own", 2, 1, 2),
+    ),
+    (
+        ("pump", 2, 1, 3), ("pump", 2, 2, 3),
+    ),
+    (),
+    (
+        ("own", 2, 1, 4), ("pump", 2, 2, 4),
+    ),
+    (
+        ("pump", 2, 2, 2), ("pump", 2, 1, 2), ("pump", 2, 1, 4), ("own", 2, 1, 3),
+    ),
+    (
+        ("pump", 2, 2, 5), ("pump", 2, 2, 1),
+    ),
+    (
+        ("pump", 2, 1, 5), ("pump", 2, 1, 1),
     ),
     (),
     (),
@@ -295,13 +295,14 @@
     def kind(piece):
         return {POOL: 0, BACK: 2}.get(piece, 1)
 
-    def z_sem(layer, k, piece):
-        return z_recv.at[layer, k, piece] if piece < 4 else z_fine.at[k, piece - 4]
+    def z_sem(layer, k, unit):
+        return z_recv.at[layer, k, unit] if unit < 5 else z_fine.at[k, unit - 5]
+
+    def own_sem(layer, k, piece):
+        return z_recv.at[layer, k, 3 + c] if piece == BACK else z_sem(layer, k, UNITS[piece][0])
 
     def amount(layer, piece):
-        if piece == BACK:
-            return 2
-        return 1 if piece == POOL else 4 / gate_cuts(layer)
+        return 1 if piece in (POOL, BACK) else 4 / gate_cuts(layer)
 
     def own_copy(layer, flow, half, piece, plane, recv):
         if piece != BACK:
@@ -324,17 +325,17 @@
         block = blocks[k]
 
         def act():
-            units(z_sem(layer, k, piece), amount(layer, piece)).wait_recv()
             for unit in UNITS[piece]:
+                units(z_sem(layer, k, unit), amount(layer, piece)).wait_recv()
                 if k == 0 and mid:
-                    w_copy(layer, 2, block, g, unit, {"sp": mid_far}, z_sem(layer, 2, piece)).start()
+                    w_copy(layer, 2, block, g, unit, {"sp": mid_far}, z_sem(layer, 2, unit)).start()
                     continue
                 w_copy(
                     layer, 2 + k, block, g, unit, {"grp": other}, y_recv.at[layer, kind(piece)]
                 ).start()
                 if mid and layer > 0:
                     w_copy(
-                        layer, 4 + k, block, g, unit, {"sp": end_here}, z_sem(layer, k, piece)
+                        layer, 4 + k, block, g, unit, {"sp": end_here}, z_sem(layer, k, unit)
                     ).start()
         holds(block, piece, act)
 
@@ -347,11 +348,11 @@
                 def _():
                     bx_copy(layer).start()
         if mid and flow == 0:
-            own_copy(layer, 0, g, piece, mid_far, z_sem(layer, 1, piece)).start()
+            own_copy(layer, 0, g, piece, mid_far, own_sem(layer, 1, piece)).start()
         elif mid:
-            own_copy(layer, 1, g, piece, end_here, z_sem(layer, 0, piece)).start()
+            own_copy(layer, 1, g, piece, end_here, own_sem(layer, 0, piece)).start()
         elif flow == 0:
-            own_copy(layer, 0, g, piece, mid_here, z_sem(layer, 0, piece)).start()
+            own_copy(layer, 0, g, piece, mid_here, own_sem(layer, 0, piece)).start()
         else:
             own_copy(layer, 1, other, piece, mid_here, y_recv.at[layer, kind(piece)]).start()
 
@@ -717,8 +718,7 @@
                 gathered[layer + 1, t, k] = state
                 start_gather(layer + 1, k)
             else:
-                final[k] = state
-                out_copy(k).start()
+                out_hbm[:, k * cols_k:(k + 1) * cols_k] = state
             relays()
 
     def sent(sem, count):
@@ -764,8 +764,6 @@
         outward = layer > 0
         halo_do(layer, 0, (s < last) if outward else (s == 1), lambda x: x.wait_send())
         halo_do(layer, 1, (s > 0) if outward else (s == 2), lambda x: x.wait_send())
-    for k in range(CHUNKS):
-        out_copy(k).wait()
 
 
 def fused(tokens_in, norm_gain, w_pool_in, w_gate, w_back):
@@ -780,9 +778,9 @@
     hbm = pl.BlockSpec(memory_space=pltpu.HBM)
     return pl.pallas_call(
         functools.partial(fused_kernel, sp_count, tp_count),
-        out_shape=jax.ShapeDtypeStruct((toks, feats), bf),
+        out_shape=pltpu.VMEM((toks, feats), bf),
         in_specs=[hbm] * 5,
-        out_specs=hbm,
+        out_specs=pl.BlockSpec(memory_space=pltpu.VMEM),
         scratch_shapes=[
             pltpu.VMEM((LAYERS, sp_count * depth, local_pool), bf),
             pltpu.VMEM((LAYERS, sp_count * depth, w_gate.shape[2]), bf),
@@ -802,7 +800,7 @@
             pltpu.VMEM(norm_gain.shape, f32),
             pltpu.VMEM((CHUNKS, toks, cols_k), bf),
             dma((LAYERS + 1, 4)),
-            dma((7,)), dma((LAYERS, 3, 4)), dma((3, 2)), dma((LAYERS, 3)),
+            dma((7,)), dma((LAYERS, 3, 5)), dma((3, 2)), dma((LAYERS, 3)),
             dma((1,)), dma((LAYERS,)),
             dma((1,)), dma((CHUNKS,)), dma((1,)), dma((CHUNKS,)),
             dma((1,)), dma((slots, 4)),

time: 98.6 us -> 96.1 us (0.975)
  Pallas kernels: 96.5 us -> 95.3 us
    pallas_call x1, Pallas kernels: 96.5 us -> 95.3 us  [fused(): pl.pallas_call(functools.partial(fused_kernel, sp_count, tp_count), out_s...]
where the time goes in v5:
time: 96.1 us; the launch traced here: 96 us
  Pallas kernels  95.3 us (99%)
    pallas_call x1, Pallas kernels, fused(): pl.pallas_call(functools.partial(fused_kernel, sp_count, tp_count), out_s...  95.3 us

profile of v5, /device:TPU:0, one launch (start us, length us, event | category | flops | bytes accessed | tf_op | source)
XLA Modules:
  0.0 96.0 jit_solution(14343456816120626159)
XLA Ops:
  0.0 95.3 %shard_map.55 = bf16[256,512]{1,0:T(8,128)(2,1)S(1)} custom-call(bf16[256,512]{1,0:T(8,128)(2,1)} %tok_hbm.1, f32[3,2048]{1,0:T(4,128)} %gain_hbm.1, bf16[3,512,256]{2,1,0:T(8,128)(2,1)} %wp_hbm.1, bf16[3,512,512]{2,1,0:T(8,128)(2,1)} %wg_hbm.1, bf16[3,256,512]{2,1,0:T(8,128)(2,1)} %wb_hbm.1), custom_call_target="tpu_custom_call" | custom-call | tf_op jit(solution)/shard_map/pallas_call | solution.py:779
  95.3 0.7 copy.7

commit v6 on v5

--- a/solution.py
+++ b/solution.py
@@ -118,57 +118,56 @@
 UNITS = {POOL: (0,), GATE_A: (1,), GATE_B: (2,), BACK: (3, 4), 4: (5,), 5: (6,)}
 GATE_PART = {1: 0, 2: 1, 5: 2, 6: 3}
 CHUNKS = 2
-GUEST = LAYERS
+GUEST, AGAIN = LAYERS, LAYERS + 1
 
 
 MID_FIRST = (
-    ("own", 1, 1, 0), ("own", 1, 0, 1), ("own", 0, 0, 2), ("own", 2, 1, 4), ("gstart", 0), ("own", 1, 1, 1),
-    ("own", 2, 1, 0), ("own", 0, 0, 0), ("own", 0, 0, 3), ("own", 2, 1, 5), ("pump", 0, 0, 3),
-    ("own", 1, 1, 3), ("own", 2, 1, 2), ("pump", 0, 0, 0), ("own", 1, 1, 2), ("pump", 1, 1, 1),
-    ("own", 0, 0, 1), ("pump", 0, 1, 0), ("guest", 0), ("pump", 0, 1, 3), ("own", 2, 1, 3),
-    ("pump", 0, 1, 2), ("guest", 1), ("agf", 0, 0), ("pump", 0, 2, 0), ("agf", 0, 1), ("pump", 0, 0, 1),
-    ("pump", 0, 0, 2), ("pump", 0, 2, 3), ("own", 2, 1, 1), ("agf", 3, 0), ("own", 1, 0, 0), ("agf", 3, 1),
-    ("pump", 0, 1, 1), ("pool", 0), ("pool", 3), ("pump", 1, 0, 3), ("pump", 0, 2, 1), ("pump", 0, 2, 2),
-    ("back", 3), ("pump", 1, 1, 0), ("box", 0), ("pump", 1, 2, 3), ("pump", 1, 0, 0), ("own", 1, 0, 3),
-    ("back", 0), ("gate", 3), ("upd", 3, 0), ("upd", 3, 1), ("own", 1, 0, 2), ("gate", 0),
-    ("pump", 1, 2, 0), ("upd", 0, 0), ("pump", 1, 0, 1), ("upd", 0, 1), ("pump", 1, 1, 3), ("own", 2, 0, 0),
-    ("pump", 1, 2, 1), ("pump", 1, 0, 2),
+    ("own", 2, 1, 4), ("own", 2, 1, 2), ("own", 0, 0, 2), ("own", 0, 0, 0), ("own", 2, 1, 5),
+    ("own", 1, 1, 0), ("pump", 0, 0, 0), ("own", 0, 0, 3), ("own", 2, 1, 0), ("pump", 0, 1, 2),
+    ("pump", 0, 0, 3), ("own", 1, 0, 0), ("pump", 0, 1, 0), ("own", 1, 1, 3), ("gstart", 0),
+    ("pump", 0, 2, 0), ("pump", 0, 1, 3), ("guest", 0), ("guest", 1), ("agf", 0, 0), ("own", 1, 0, 3),
+    ("agf", 0, 1), ("pump", 0, 2, 3), ("pool", 0), ("pump", 0, 0, 2), ("own", 0, 0, 1), ("agf", 3, 0),
+    ("pump", 1, 1, 0), ("pump", 0, 0, 1), ("own", 2, 0, 1), ("pump", 1, 1, 3), ("agf", 3, 1),
+    ("own", 2, 1, 1), ("pool", 3), ("pump", 1, 0, 0), ("own", 1, 0, 1), ("own", 2, 1, 3), ("pump", 0, 2, 2),
+    ("back", 3), ("pump", 0, 1, 1), ("box", 0), ("pump", 0, 2, 1), ("back", 0), ("pump", 2, 1, 1),
+    ("pump", 1, 2, 0), ("own", 1, 0, 2), ("pump", 1, 0, 3), ("gate", 3), ("gate", 0), ("upd", 0, 0),
+    ("upd", 0, 1), ("pump", 1, 1, 1), ("pump", 1, 0, 2), ("upd", 3, 0), ("upd", 3, 1), ("pump", 1, 1, 2),
+    ("own", 2, 0, 2), ("pump", 1, 0, 1),
 )
 END_FIRST = (
-    ("own", 0, 0, 0), ("own", 0, 0, 3), ("tok", 0), ("tok", 1), ("own", 0, 1, 0), ("own", 0, 0, 1),
-    ("own", 0, 0, 2), ("own", 0, 1, 3), ("own", 1, 0, 3), ("own", 1, 0, 0), ("own", 0, 1, 2),
-    ("own", 0, 1, 1), ("own", 1, 0, 1), ("own", 1, 0, 2), ("pump", 1, 0, 0), ("own", 1, 1, 0),
-    ("own", 2, 0, 3), ("pump", 2, 0, 5), ("own", 2, 0, 0), ("pump", 1, 0, 2), ("pump", 1, 1, 1),
-    ("own", 1, 1, 3), ("pump", 2, 0, 2), ("pump", 1, 0, 3), ("pump", 1, 0, 1), ("pump", 2, 0, 3),
-    ("pump", 2, 0, 4), ("own", 2, 0, 4), ("own", 2, 0, 2), ("pump", 1, 2, 3), ("ret", 0), ("pump", 2, 0, 0),
-    ("pump", 1, 1, 0), ("ret", 1), ("pump", 1, 2, 0),
+    ("own", 0, 0, 0), ("own", 0, 0, 3), ("tok", 0), ("tok", 1), ("own", 0, 1, 0), ("own", 0, 0, 2),
+    ("own", 0, 0, 1), ("own", 1, 0, 0), ("own", 0, 1, 3), ("own", 0, 1, 1), ("own", 1, 0, 3),
+    ("own", 0, 1, 2), ("pump", 1, 1, 0), ("own", 1, 0, 2), ("own", 1, 0, 1), ("pump", 2, 0, 5),
+    ("pump", 2, 0, 4), ("pump", 2, 0, 0), ("pump", 2, 0, 2), ("pump", 1, 0, 0), ("pump", 1, 2, 0),
+    ("own", 2, 0, 3), ("own", 1, 1, 0), ("own", 1, 1, 2), ("ret", 0), ("own", 1, 1, 1), ("pump", 1, 1, 3),
+    ("ret", 1),
 )
 MID_REST = (
-    (),
-    (),
-    (
-        ("pump", 2, 0, 0), ("pump", 2, 0, 3), ("pump", 1, 2, 2), ("pump", 1, 1, 2), ("own", 2, 0, 5),
-        ("own", 2, 0, 3),
-    ),
-    (
-        ("pump", 2, 1, 0),
-    ),
-    (
-        ("pump", 2, 2, 0), ("pump", 2, 2, 3), ("pump", 2, 0, 2), ("own", 2, 0, 2), ("pump", 2, 0, 4),
-        ("own", 2, 0, 4), ("pump", 2, 1, 3),
-    ),
-    (),
-    (),
-    (
-        ("pump", 2, 2, 4), ("pump", 2, 0, 5), ("own", 2, 0, 1), ("pump", 2, 0, 1), ("pump", 2, 2, 2),
-        ("pump", 2, 1, 2),
-    ),
-    (
-        ("pump", 2, 1, 4),
-    ),
-    (),
-    (
-        ("pump", 2, 2, 5), ("pump", 2, 2, 1), ("pump", 2, 1, 5), ("pump", 2, 1, 1),
+    (
+        ("pump", 1, 2, 3), ("pump", 1, 2, 2),
+    ),
+    (
+        ("pump", 2, 1, 2), ("pump", 2, 0, 3), ("pump", 1, 2, 1),
+    ),
+    (
+        ("agf", 4, 0), ("agf", 4, 1), ("own", 2, 0, 0), ("pump", 2, 2, 3), ("gate", 4), ("pump", 2, 0, 0),
+    ),
+    (),
+    (
+        ("own", 2, 0, 3), ("pump", 2, 2, 0), ("pump", 2, 1, 0), ("own", 2, 0, 5),
+    ),
+    (),
+    (
+        ("pump", 2, 1, 5),
+    ),
+    (
+        ("pump", 2, 0, 2), ("pump", 2, 0, 5), ("pump", 2, 1, 3), ("pump", 2, 2, 5), ("pump", 2, 0, 1),
+        ("pump", 2, 0, 4), ("pump", 2, 2, 2), ("own", 2, 0, 4),
+    ),
+    (),
+    (),
+    (
+        ("pump", 2, 1, 4), ("pump", 2, 2, 4), ("pump", 2, 2, 1),
     ),
     (),
     (),
@@ -178,53 +177,50 @@
 )
 END_REST = (
     (
-        ("pump", 1, 1, 3), ("pump", 2, 0, 1),
-    ),
-    (),
-    (
-        ("pump", 1, 2, 1), ("own", 1, 1, 2),
-    ),
-    (
-        ("pump", 1, 2, 2), ("own", 1, 1, 1),
-    ),
-    (
-        ("own", 2, 1, 1), ("pump", 1, 1, 2), ("own", 2, 0, 5), ("own", 2, 0, 1), ("pump", 2, 1, 0),
-        ("own", 2, 1, 5),
-    ),
-    (),
-    (
-        ("pump", 2, 2, 0), ("own", 2, 1, 0), ("own", 2, 1, 2),
-    ),
-    (
-        ("pump", 2, 1, 3), ("pump", 2, 2, 3),
-    ),
-    (),
-    (
-        ("own", 2, 1, 4), ("pump", 2, 2, 4),
-    ),
-    (
-        ("pump", 2, 2, 2), ("pump", 2, 1, 2), ("pump", 2, 1, 4), ("own", 2, 1, 3),
-    ),
-    (
-        ("pump", 2, 2, 5), ("pump", 2, 2, 1),
-    ),
-    (
-        ("pump", 2, 1, 5), ("pump", 2, 1, 1),
+        ("pump", 1, 0, 3), ("pump", 2, 0, 3), ("own", 2, 0, 0),
+    ),
+    (),
+    (
+        ("own", 1, 1, 3), ("own", 2, 0, 1), ("pump", 1, 2, 3), ("own", 2, 0, 5),
+    ),
+    (
+        ("own", 2, 0, 4),
+    ),
+    (
+        ("own", 2, 0, 2), ("pump", 2, 1, 1), ("pump", 2, 1, 2), ("pump", 2, 2, 3), ("pump", 2, 0, 1),
+        ("own", 2, 1, 4),
+    ),
+    (),
+    (),
+    (
+        ("own", 2, 1, 3), ("pump", 2, 2, 0), ("own", 2, 1, 0), ("pump", 2, 1, 0),
+    ),
+    (),
+    (
+        ("own", 2, 1, 1), ("pump", 2, 1, 3), ("pump", 2, 1, 5),
+    ),
+    (
+        ("own", 2, 1, 2), ("pump", 2, 2, 5), ("pump", 2, 2, 2),
+    ),
+    (),
+    (
+        ("pump", 2, 1, 4), ("pump", 2, 2, 4), ("own", 2, 1, 5), ("pump", 2, 2, 1),
     ),
     (),
     (),
     (),
 )
+AGAIN_FIRST = True
 FIRST_BACK, FIRST_GATE = 3, 3
 
 
 def fused_kernel(
     sp_count, tp_count,
-    tok_hbm, gain_hbm, wp_hbm, wg_hbm, wb_hbm, out_hbm,
+    tok_hbm, gain_hbm, wp_hbm, wg_hbm, wb_hbm, out_ref,
     wp, wg, wb, wb_own, gathered, scaled, halo, gate_buf, own_part, box, counts,
-    pair, parts, arrived, returned, gain_ref, final,
+    pair, parts, arrived, gate_sent, gain_ref,
     load_sem, w_send, z_recv, z_fine, y_recv, bx_send, bx_recv, tk_send, tk_recv, rt_send, rt_recv,
-    ag_send, ag_recv, h_send, h_recv, px_send, px_recv, rs_send, rs_recv,
+    ag_send, ag_recv, h_send, h_recv, px_send, px_recv, rs_send, rs_recv, gv_send, gv_recv,
 ):
     g = lax.axis_index("grp")
     s = lax.axis_index("sp")
@@ -333,7 +329,7 @@
                 w_copy(
                     layer, 2 + k, block, g, unit, {"grp": other}, y_recv.at[layer, kind(piece)]
                 ).start()
-                if mid and layer > 0:
+                if mid and layer > 0 and (layer, kind(piece)) != (1, 1):
                     w_copy(
                         layer, 4 + k, block, g, unit, {"sp": end_here}, z_sem(layer, k, unit)
                     ).start()
@@ -402,11 +398,6 @@
 
     gain_load = pltpu.make_async_copy(gain_hbm, gain_ref, load_sem.at[LAYERS, CHUNKS])
 
-    def out_copy(k):
-        return pltpu.make_async_copy(
-            final.at[k], out_hbm.at[:, pl.ds(k * cols_k, cols_k)], load_sem.at[0, k]
-        )
-
     def guest_copy(k):
         return pltpu.make_async_remote_copy(
             src_ref=gathered.at[0, t, k], dst_ref=gathered.at[GUEST, t, k],
@@ -416,7 +407,7 @@
 
     def return_copy(k):
         return pltpu.make_async_remote_copy(
-            src_ref=returned.at[k], dst_ref=gathered.at[1, t, k],
+            src_ref=gathered.at[AGAIN, t, k], dst_ref=gathered.at[1, t, k],
             send_sem=rt_send.at[0], recv_sem=rt_recv.at[k],
             device_id={"sp": end_here}, device_id_type=MESH,
         )
@@ -591,8 +582,32 @@
     def relay(mid, item):
         if item[0] == "own":
             own(mid, waited_mid if mid else waited_end, *item[1:])
+        elif item[0] == "agf":
+            pass_on(AGAIN, item[2])
+        elif item[0] == "gate":
+            again_gate()
         else:
             pump(mid, *item[1:])
+
+    def gate_copy(k):
+        return pltpu.make_async_remote_copy(
+            src_ref=gate_sent.at[k], dst_ref=gate_sent.at[k],
+            send_sem=gv_send.at[0], recv_sem=gv_recv.at[0],
+            device_id={"sp": end_here}, device_id_type=MESH,
+        )
+
+    def again_gate():
+        for which in (3, 2):
+            units(ag_recv.at[AGAIN, which], 2).wait_recv()
+        total = zero
+        for block in (t, t1, t2, t3):
+            total = absorb(1, AGAIN, 1, block, total)
+        if AGAIN_FIRST:
+            ready(1, 1)
+        gate_of(1, 1, scale_of(total))
+        for k in range(CHUNKS):
+            gate_sent[k] = gate_buf[1, k].astype(bf)
+            gate_copy(k).start()
 
     def gather_step(layer, slot, which, k, total):
         if k == 0:
@@ -673,8 +688,9 @@
                 k = item[2]
                 value = update(slot, which, k)
                 if slot == GUEST:
-                    returned[k] = value
+                    gathered[AGAIN, t, k] = value
                     return_copy(k).start()
+                    start_gather(AGAIN, k)
                 else:
                     gathered[1, t, k] = value
                     start_gather(1, k)
@@ -709,8 +725,21 @@
         ready(layer, 2)
         back(layer, layer, 0)
         relays()
-        ready(layer, 1)
-        gate_of(layer, 0, scale)
+        if layer == 1:
+            @pl.when(is_mid)
+            def _(scale=scale):
+                if not AGAIN_FIRST:
+                    ready(1, 1)
+                gate_of(1, 0, scale)
+
+            @pl.when(is_end)
+            def _():
+                units(gv_recv.at[0], CHUNKS).wait_recv()
+                for k in range(CHUNKS):
+                    gate_buf[0, k] = gate_sent[k].astype(f32)
+        else:
+            ready(layer, 1)
+            gate_of(layer, 0, scale)
         relays()
         for k in range(CHUNKS):
             state = update(layer, 0, k)
@@ -718,48 +747,49 @@
                 gathered[layer + 1, t, k] = state
                 start_gather(layer + 1, k)
             else:
-                out_hbm[:, k * cols_k:(k + 1) * cols_k] = state
+                out_ref[:, k * cols_k:(k + 1) * cols_k] = state
             relays()
 
     def sent(sem, count):
         units(sem, count).wait_send()
 
-    def sent_blocks(flow, k, layers):
+    def sent_blocks(flow, k, most, least):
         @pl.when(c == blocks[k] % 2)
         def _():
-            sent(w_send.at[flow], 5 * layers)
+            sent(w_send.at[flow], most)
 
         @pl.when(c != blocks[k] % 2)
         def _():
-            sent(w_send.at[flow], 3 * layers)
-
-    def sent_chain(layers, slots):
+            sent(w_send.at[flow], least)
+
+    def sent_chain(layers, slots, gathers):
         @pl.when(c != s_parity)
         def _():
             sent(bx_send.at[0], 2 * layers)
-        sent(ag_send.at[0], 6 * slots)
+        sent(ag_send.at[0], 6 * gathers)
         sent(rs_send.at[0], 2 * slots)
         sent(px_send.at[0], slots)
 
     @pl.when(is_mid)
     def _():
         sent(w_send.at[0], 4 * LAYERS)
-        sent(w_send.at[1], 4 * (LAYERS - 1))
+        sent(w_send.at[1], 4 * (LAYERS - 1) - 2)
         for k in range(3):
-            sent_blocks(2 + k, k, LAYERS)
+            sent_blocks(2 + k, k, 5 * LAYERS, 3 * LAYERS)
         for k in (1, 2):
-            sent_blocks(4 + k, k, LAYERS - 1)
+            sent_blocks(4 + k, k, 5 * (LAYERS - 1) - 2, 3 * (LAYERS - 1) - 2)
         sent(rt_send.at[0], CHUNKS)
-        sent_chain(LAYERS, LAYERS + 1)
+        sent(gv_send.at[0], CHUNKS)
+        sent_chain(LAYERS, LAYERS + 1, LAYERS + 2)
 
     @pl.when(is_end)
     def _():
         sent(w_send.at[0], 4 * LAYERS)
         sent(w_send.at[1], 4 * LAYERS)
         for k in range(3):
-            sent_blocks(2 + k, k, LAYERS - 1)
+            sent_blocks(2 + k, k, 5 * (LAYERS - 1) - 2, 3 * (LAYERS - 1) - 2)
         sent(tk_send.at[0], CHUNKS)
-        sent_chain(LAYERS - 1, LAYERS - 1)
+        sent_chain(LAYERS - 1, LAYERS - 1, LAYERS - 1)
     for layer in range(LAYERS):
         outward = layer > 0
         halo_do(layer, 0, (s < last) if outward else (s == 1), lambda x: x.wait_send())
@@ -786,7 +816,7 @@
             pltpu.VMEM((LAYERS, sp_count * depth, w_gate.shape[2]), bf),
             pltpu.VMEM((LAYERS, 2, 2 * b_rows, b_cols), bf),
             pltpu.VMEM((LAYERS, b_rows, b_cols), bf),
-            pltpu.VMEM((slots, tp_count, CHUNKS, toks, cols_k), bf),
+            pltpu.VMEM((slots + 1, tp_count, CHUNKS, toks, cols_k), bf),
             pltpu.VMEM((2, toks, tp_count * feats), bf),
             pltpu.VMEM((LAYERS, 3, toks, local_pool), bf),
             pltpu.VMEM((2, CHUNKS, toks, cols_k), f32),
@@ -798,15 +828,15 @@
             pltpu.VMEM((slots, CHUNKS, toks, cols_k), bf),
             pltpu.VMEM((CHUNKS, toks, cols_k), bf),
             pltpu.VMEM(norm_gain.shape, f32),
-            pltpu.VMEM((CHUNKS, toks, cols_k), bf),
             dma((LAYERS + 1, 4)),
             dma((7,)), dma((LAYERS, 3, 5)), dma((3, 2)), dma((LAYERS, 3)),
             dma((1,)), dma((LAYERS,)),
             dma((1,)), dma((CHUNKS,)), dma((1,)), dma((CHUNKS,)),
-            dma((1,)), dma((slots, 4)),
+            dma((1,)), dma((slots + 1, 4)),
             dma((LAYERS, 2)), dma((LAYERS, 2)),
             dma((1,)), dma((slots,)),
             dma((1,)), dma((slots, CHUNKS)),
+            dma((1,)), dma((1,)),
         ],
         compiler_params=pltpu.CompilerParams(
             collective_id=0, has_side_effects=True, vmem_limit_bytes=56 * 1024 * 1024

time: 96.1 us -> 95.3 us (level)
  Pallas kernels: 95.3 us -> 94.3 us
    pallas_call x1, Pallas kernels: 95.3 us -> 94.3 us  [fused(): pl.pallas_call(functools.partial(fused_kernel, sp_count, tp_count), out_s...]
where the time goes in v6:
time: 95.3 us; the launch traced here: 95 us
  Pallas kernels  94.3 us (99%)
    pallas_call x1, Pallas kernels, fused(): pl.pallas_call(functools.partial(fused_kernel, sp_count, tp_count), out_s...  94.3 us

profile of v6, /device:TPU:0, one launch (start us, length us, event | category | flops | bytes accessed | tf_op | source)
XLA Modules:
  0.0 95.0 jit_solution(3195508943806659547)
XLA Ops:
  0.0 94.3 %shard_map.55 = bf16[256,512]{1,0:T(8,128)(2,1)S(1)} custom-call(bf16[256,512]{1,0:T(8,128)(2,1)} %tok_hbm.1, f32[3,2048]{1,0:T(4,128)} %gain_hbm.1, bf16[3,512,256]{2,1,0:T(8,128)(2,1)} %wp_hbm.1, bf16[3,512,512]{2,1,0:T(8,128)(2,1)} %wg_hbm.1, bf16[3,256,512]{2,1,0:T(8,128)(2,1)} %wb_hbm.1), custom_call_target="tpu_custom_call" | custom-call | tf_op jit(solution)/shard_map/pallas_call | solution.py:809
  94.3 0.7 copy.7

commit v7 on v6

--- a/solution.py
+++ b/solution.py
@@ -122,50 +122,51 @@
 
 
 MID_FIRST = (
-    ("own", 2, 1, 4), ("own", 2, 1, 2), ("own", 0, 0, 2), ("own", 0, 0, 0), ("own", 2, 1, 5),
-    ("own", 1, 1, 0), ("pump", 0, 0, 0), ("own", 0, 0, 3), ("own", 2, 1, 0), ("pump", 0, 1, 2),
-    ("pump", 0, 0, 3), ("own", 1, 0, 0), ("pump", 0, 1, 0), ("own", 1, 1, 3), ("gstart", 0),
-    ("pump", 0, 2, 0), ("pump", 0, 1, 3), ("guest", 0), ("guest", 1), ("agf", 0, 0), ("own", 1, 0, 3),
-    ("agf", 0, 1), ("pump", 0, 2, 3), ("pool", 0), ("pump", 0, 0, 2), ("own", 0, 0, 1), ("agf", 3, 0),
-    ("pump", 1, 1, 0), ("pump", 0, 0, 1), ("own", 2, 0, 1), ("pump", 1, 1, 3), ("agf", 3, 1),
-    ("own", 2, 1, 1), ("pool", 3), ("pump", 1, 0, 0), ("own", 1, 0, 1), ("own", 2, 1, 3), ("pump", 0, 2, 2),
-    ("back", 3), ("pump", 0, 1, 1), ("box", 0), ("pump", 0, 2, 1), ("back", 0), ("pump", 2, 1, 1),
-    ("pump", 1, 2, 0), ("own", 1, 0, 2), ("pump", 1, 0, 3), ("gate", 3), ("gate", 0), ("upd", 0, 0),
-    ("upd", 0, 1), ("pump", 1, 1, 1), ("pump", 1, 0, 2), ("upd", 3, 0), ("upd", 3, 1), ("pump", 1, 1, 2),
-    ("own", 2, 0, 2), ("pump", 1, 0, 1),
+    ("own", 2, 1, 0), ("own", 2, 1, 2), ("own", 0, 0, 0), ("own", 0, 0, 2), ("gstart", 0),
+    ("pump", 0, 1, 0), ("pump", 0, 0, 0), ("own", 0, 0, 3), ("guest", 0), ("pump", 0, 1, 2),
+    ("own", 2, 1, 4), ("pump", 0, 2, 0), ("pump", 0, 0, 3), ("pump", 0, 1, 3), ("own", 1, 0, 3),
+    ("agf", 0, 0), ("own", 1, 1, 3), ("agf", 0, 1), ("own", 1, 1, 0), ("own", 1, 0, 0), ("own", 2, 1, 3),
+    ("guest", 1), ("pump", 0, 2, 3), ("pool", 0), ("pump", 0, 0, 2), ("pump", 1, 1, 0), ("agf", 3, 0),
+    ("agf", 3, 1), ("own", 0, 0, 1), ("pump", 0, 0, 1), ("pump", 1, 1, 3), ("pool", 3), ("box", 0),
+    ("own", 2, 1, 1), ("own", 2, 1, 5), ("own", 2, 0, 1), ("pump", 1, 0, 0), ("pump", 0, 2, 2), ("back", 3),
+    ("own", 1, 0, 1), ("pump", 0, 1, 1), ("own", 1, 0, 2), ("back", 0), ("pump", 0, 2, 1),
+    ("pump", 2, 1, 1), ("pump", 1, 2, 0), ("gate", 3), ("pump", 1, 0, 3), ("gate", 0), ("upd", 0, 0),
+    ("upd", 0, 1), ("upd", 3, 0), ("upd", 3, 1), ("pump", 1, 0, 2), ("own", 2, 0, 2), ("pump", 1, 1, 1),
+    ("pump", 1, 0, 1), ("pump", 1, 1, 2), ("pump", 1, 2, 3),
 )
 END_FIRST = (
-    ("own", 0, 0, 0), ("own", 0, 0, 3), ("tok", 0), ("tok", 1), ("own", 0, 1, 0), ("own", 0, 0, 2),
-    ("own", 0, 0, 1), ("own", 1, 0, 0), ("own", 0, 1, 3), ("own", 0, 1, 1), ("own", 1, 0, 3),
-    ("own", 0, 1, 2), ("pump", 1, 1, 0), ("own", 1, 0, 2), ("own", 1, 0, 1), ("pump", 2, 0, 5),
-    ("pump", 2, 0, 4), ("pump", 2, 0, 0), ("pump", 2, 0, 2), ("pump", 1, 0, 0), ("pump", 1, 2, 0),
-    ("own", 2, 0, 3), ("own", 1, 1, 0), ("own", 1, 1, 2), ("ret", 0), ("own", 1, 1, 1), ("pump", 1, 1, 3),
+    ("own", 0, 0, 0), ("tok", 0), ("own", 0, 0, 3), ("own", 0, 1, 0), ("tok", 1), ("own", 0, 0, 2),
+    ("own", 0, 0, 1), ("own", 1, 0, 0), ("own", 0, 1, 3), ("own", 0, 1, 2), ("own", 0, 1, 1),
+    ("own", 1, 0, 2), ("own", 1, 0, 3), ("own", 1, 0, 1), ("own", 1, 1, 2), ("pump", 1, 0, 0),
+    ("pump", 1, 1, 0), ("own", 2, 0, 3), ("pump", 1, 1, 3), ("pump", 2, 0, 2), ("pump", 1, 0, 3),
+    ("pump", 2, 0, 0), ("own", 1, 1, 0), ("own", 1, 1, 1), ("pump", 1, 2, 0), ("pump", 2, 0, 5), ("ret", 0),
     ("ret", 1),
 )
 MID_REST = (
     (
-        ("pump", 1, 2, 3), ("pump", 1, 2, 2),
-    ),
-    (
-        ("pump", 2, 1, 2), ("pump", 2, 0, 3), ("pump", 1, 2, 1),
-    ),
-    (
-        ("agf", 4, 0), ("agf", 4, 1), ("own", 2, 0, 0), ("pump", 2, 2, 3), ("gate", 4), ("pump", 2, 0, 0),
-    ),
-    (),
-    (
-        ("own", 2, 0, 3), ("pump", 2, 2, 0), ("pump", 2, 1, 0), ("own", 2, 0, 5),
-    ),
-    (),
-    (
-        ("pump", 2, 1, 5),
-    ),
-    (
-        ("pump", 2, 0, 2), ("pump", 2, 0, 5), ("pump", 2, 1, 3), ("pump", 2, 2, 5), ("pump", 2, 0, 1),
-        ("pump", 2, 0, 4), ("pump", 2, 2, 2), ("own", 2, 0, 4),
-    ),
-    (),
-    (),
+        ("pump", 1, 2, 2), ("pump", 2, 0, 3),
+    ),
+    (
+        ("pump", 2, 1, 2), ("pump", 1, 2, 1), ("agf", 4, 0),
+    ),
+    (
+        ("own", 2, 0, 0), ("agf", 4, 1), ("pump", 2, 2, 3), ("gate", 4), ("pump", 2, 0, 0),
+        ("own", 2, 0, 3),
+    ),
+    (),
+    (),
+    (
+        ("pump", 2, 2, 0), ("own", 2, 0, 5), ("pump", 2, 0, 1), ("pump", 2, 1, 0),
+    ),
+    (),
+    (
+        ("pump", 2, 0, 5), ("pump", 2, 1, 3), ("pump", 2, 1, 5), ("pump", 2, 0, 2), ("pump", 2, 2, 2),
+        ("pump", 2, 0, 4),
+    ),
+    (),
+    (
+        ("pump", 2, 2, 5), ("own", 2, 0, 4),
+    ),
     (
         ("pump", 2, 1, 4), ("pump", 2, 2, 4), ("pump", 2, 2, 1),
     ),
@@ -177,34 +178,40 @@
 )
 END_REST = (
     (
-        ("pump", 1, 0, 3), ("pump", 2, 0, 3), ("own", 2, 0, 0),
-    ),
-    (),
-    (
-        ("own", 1, 1, 3), ("own", 2, 0, 1), ("pump", 1, 2, 3), ("own", 2, 0, 5),
-    ),
-    (
-        ("own", 2, 0, 4),
-    ),
-    (
-        ("own", 2, 0, 2), ("pump", 2, 1, 1), ("pump", 2, 1, 2), ("pump", 2, 2, 3), ("pump", 2, 0, 1),
-        ("own", 2, 1, 4),
-    ),
-    (),
-    (),
-    (
-        ("own", 2, 1, 3), ("pump", 2, 2, 0), ("own", 2, 1, 0), ("pump", 2, 1, 0),
-    ),
-    (),
-    (
-        ("own", 2, 1, 1), ("pump", 2, 1, 3), ("pump", 2, 1, 5),
-    ),
-    (
-        ("own", 2, 1, 2), ("pump", 2, 2, 5), ("pump", 2, 2, 2),
-    ),
-    (),
-    (
-        ("pump", 2, 1, 4), ("pump", 2, 2, 4), ("own", 2, 1, 5), ("pump", 2, 2, 1),
+        ("pump", 2, 0, 4), ("pump", 2, 1, 1),
+    ),
+    (
+        ("pump", 1, 2, 3), ("own", 2, 0, 0),
+    ),
+    (
+        ("own", 1, 1, 3), ("own", 2, 0, 4), ("pump", 2, 0, 3), ("own", 2, 0, 5), ("own", 2, 0, 1),
+        ("own", 2, 0, 2), ("pump", 2, 1, 2),
+    ),
+    (
+        ("pump", 2, 2, 3), ("own", 2, 1, 2), ("own", 2, 1, 3),
+    ),
+    (
+        ("own", 2, 1, 0),
+    ),
+    (),
+    (
+        ("own", 2, 1, 5), ("pump", 2, 0, 1), ("own", 2, 1, 4),
+    ),
+    (
+        ("pump", 2, 2, 0), ("pump", 2, 1, 0),
+    ),
+    (),
+    (
+        ("pump", 2, 1, 3),
+    ),
+    (
+        ("pump", 2, 1, 5), ("pump", 2, 2, 2),
+    ),
+    (
+        ("pump", 2, 2, 5),
+    ),
+    (
+        ("own", 2, 1, 1), ("pump", 2, 1, 4), ("pump", 2, 2, 4), ("pump", 2, 2, 1),
     ),
     (),
     (),

time: 95.3 us -> 96.3 us (1.010)
  Pallas kernels: 94.3 us -> 95.4 us
    pallas_call x1, Pallas kernels: 94.3 us -> 95.4 us  [fused(): pl.pallas_call(functools.partial(fused_kernel, sp_count, tp_count), out_s...]
where the time goes in v7:
time: 96.3 us; the launch traced here: 96.2 us
  Pallas kernels  95.4 us (99%)
    pallas_call x1, Pallas kernels, fused(): pl.pallas_call(functools.partial(fused_kernel, sp_count, tp_count), out_s...  95.4 us

profile of v7, /device:TPU:0, one launch (start us, length us, event | category | flops | bytes accessed | tf_op | source)
XLA Modules:
  0.0 96.2 jit_solution(8197439942393810963)
XLA Ops:
  0.0 95.4 %shard_map.55 = bf16[256,512]{1,0:T(8,128)(2,1)S(1)} custom-call(bf16[256,512]{1,0:T(8,128)(2,1)} %tok_hbm.1, f32[3,2048]{1,0:T(4,128)} %gain_hbm.1, bf16[3,512,256]{2,1,0:T(8,128)(2,1)} %wp_hbm.1, bf16[3,512,512]{2,1,0:T(8,128)(2,1)} %wg_hbm.1, bf16[3,256,512]{2,1,0:T(8,128)(2,1)} %wb_hbm.1), custom_call_target="tpu_custom_call" | custom-call | tf_op jit(solution)/shard_map/pallas_call | solution.py:816
  95.5 0.7 copy.7
